TPU v7x, 32 devices: a whole 2x2x4 slice. The times are simulated.
32 devices in a mesh: tp: 4 (over z), dp: 8 (over y, x, core).
Axes of the slice: x: 2, y: 2, z: 4, core: 2. Of those that a mesh axis runs over, the one named last changes fastest.
Arguments:
- tokens: bfloat16 [64, 4096], P(None, 'dp'), may hold values from -6 to 6
- norm_gain: float32 [2, 4096], P(None, 'dp'), may hold values from 0.1 to 1.9
- w_gate: bfloat16 [2, 4096, 3072], P(None, 'dp', 'tp'), may hold values from -0.09375 to 0.09375
- w_value: bfloat16 [2, 4096, 3072], P(None, 'dp', 'tp'), may hold values from -0.09375 to 0.09375
- w_inmap: bfloat16 [2, 4096, 3072], P(None, 'dp', 'tp'), may hold values from -0.09375 to 0.09375
- w_readout: bfloat16 [2, 4096, 3072], P(None, 'dp', 'tp'), may hold values from -0.09375 to 0.09375
- w_step: bfloat16 [2, 4096, 48], P(None, 'dp'), may hold values from -0.09375 to 0.09375
- step_bias: float32 [2, 48], P(None, 'tp'), may hold values from -4 to 1
- decay_log: float32 [2, 48], P(None, 'tp'), may hold values from -1 to 2.5
- skip_gain: float32 [2, 48], P(None, 'tp'), may hold values from 0.5 to 2
- conv_taps: bfloat16 [2, 5, 3, 3072], P(None, None, None, 'tp'), may hold values from -2.5 to 2.5
- gate_gain: float32 [2, 3072], P(None, 'tp'), may hold values from 0.1 to 1.9
- w_project: bfloat16 [2, 3072, 4096], P(None, 'tp', 'dp'), may hold values from -0.109375 to 0.109375
- states: float32 [2, 64, 48, 4096], P(None, 'dp', 'tp'), may hold values from -3 to 3
- recent: bfloat16 [2, 64, 4, 3, 3072], P(None, 'dp', None, None, 'tp'), may hold values from -6 to 6
Outputs:
- next_tokens: bfloat16 [64, 4096], P(None, 'dp')
- next_states: float32 [2, 64, 48, 4096], P(None, 'dp', 'tp')
- next_recent: bfloat16 [2, 64, 4, 3, 3072], P(None, 'dp', None, None, 'tp')
All inputs are finite; a program needn't handle non-finite values.
Results may differ from a plain program's by a relative error of at most 0.014.
Values may be sent and summed in bfloat16 or wider, within the bound.
A program may use at most 64 MiB of HBM per device.

v0:
```python
import functools

import jax
import jax.numpy as jnp
from jax import lax
from jax.experimental import pallas as pl
from jax.experimental.pallas import tpu as pltpu
from jax.sharding import PartitionSpec as P

EPS = 1e-06
LANES = 128
MESH = pl.DeviceIdType.MESH
F32 = jnp.float32
BF16 = jnp.bfloat16


def each(count, body):
    if count <= 8:
        for index in range(count):
            body(index)
    else:
        lax.fori_loop(0, count, lambda index, carry: (body(index), carry)[1], 0)


def fold(count, body, start):
    if count <= 8:
        for index in range(count):
            start = body(index, start)
        return start
    return lax.fori_loop(0, count, body, start)


def silu(value):
    return value / (1.0 + jnp.exp(-value))


def halves(value):
    high = value.astype(BF16)
    return high, (value - high.astype(F32)).astype(BF16)


def kernel(
    dims,
    tokens_ref,
    norm_ref,
    bias_ref,
    rate_ref,
    skip_ref,
    gain_ref,
    taps_ref,
    recent_ref,
    value_hbm,
    inmap_hbm,
    readout_hbm,
    gate_hbm,
    step_hbm,
    project_hbm,
    states_hbm,
    tokens_out,
    fresh_out,
    u_out,
    w_in,
    w_step,
    w_out,
    state,
    spread,
    gather,
    part_send,
    part_recv,
    extra_send,
    extra_recv,
    gated_all,
    mixed_all,
    square_all,
    conv_ref,
    params_ref,
    chosen_ref,
    dec_ref,
    bm_ref,
    cm_ref,
    wide_ref,
    x_ref,
    in_sem,
    step_sem,
    out_sem,
    state_sem,
    part_ssem,
    part_rsem,
    extra_ssem,
    extra_rsem,
    gated_ssem,
    gated_rsem,
    mixed_ssem,
    mixed_rsem,
    square_ssem,
    square_rsem,
):
    layers, dp, tp, own, cols, heads, head_dim, span, features, width = dims
    me = lax.axis_index("dp")
    col = lax.axis_index("tp")
    rows = dp * own

    def peer(k):
        return lax.rem(me + k + 1, dp)

    def column(k):
        return lax.rem(col + k + 1, tp)

    barrier = pltpu.get_barrier_semaphore()
    each(dp - 1, lambda k: pl.semaphore_signal(
        barrier, inc=1, device_id={"dp": peer(k)}, device_id_type=MESH))
    each(tp - 1, lambda k: pl.semaphore_signal(
        barrier, inc=1, device_id={"tp": column(k)}, device_id_type=MESH))

    sources = (inmap_hbm, readout_hbm, value_hbm, gate_hbm)

    def load_step(level):
        return pltpu.make_async_copy(step_hbm.at[level], w_step.at[level, : step_hbm.shape[1]], step_sem.at[level])

    def load_in(level, w):
        return pltpu.make_async_copy(
            sources[w].at[level], w_in.at[level, w], in_sem.at[level, w])

    def load_out(level):
        return pltpu.make_async_copy(project_hbm.at[level], w_out.at[level], out_sem.at[level])

    def load_state(level):
        return pltpu.make_async_copy(states_hbm.at[level], state.at[level], state_sem.at[level])

    filled = step_hbm.shape[1]
    w_step[:, filled:] = jnp.zeros((layers, LANES - filled, width), BF16)
    for level in range(layers):
        load_step(level).start()
        for w in range(4):
            load_in(level, w).start()
        load_state(level).start()
        load_out(level).start()

    def send_extra(level, k):
        return pltpu.make_async_remote_copy(
            src_ref=extra_send.at[level, peer(k)],
            dst_ref=extra_recv.at[level, k],
            send_sem=extra_ssem.at[level, k],
            recv_sem=extra_rsem.at[level, k],
            device_id={"dp": peer(k)},
            device_id_type=MESH,
        )

    def send_part(level, w, k):
        return pltpu.make_async_remote_copy(
            src_ref=part_send.at[level, w, peer(k)],
            dst_ref=part_recv.at[level, w, k],
            send_sem=part_ssem.at[level, w, k],
            recv_sem=part_rsem.at[level, w, k],
            device_id={"dp": peer(k)},
            device_id_type=MESH,
        )

    def send_gated(level, k):
        return pltpu.make_async_remote_copy(
            src_ref=gated_all.at[level, me],
            dst_ref=gated_all.at[level, me],
            send_sem=gated_ssem.at[level, k],
            recv_sem=gated_rsem.at[level, k],
            device_id={"dp": peer(k)},
            device_id_type=MESH,
        )

    def send_mixed(level, k):
        return pltpu.make_async_remote_copy(
            src_ref=mixed_all.at[level, col],
            dst_ref=mixed_all.at[level, col],
            send_sem=mixed_ssem.at[level, k],
            recv_sem=mixed_rsem.at[level, k],
            device_id={"tp": column(k)},
            device_id_type=MESH,
        )

    def send_square(level, k):
        return pltpu.make_async_remote_copy(
            src_ref=square_all.at[level, col],
            dst_ref=square_all.at[level, col],
            send_sem=square_ssem.at[level, k],
            recv_sem=square_rsem.at[level, k],
            device_id={"tp": column(k)},
            device_id_type=MESH,
        )

    x_ref[...] = tokens_ref[...].astype(F32)
    lane_all = lax.broadcasted_iota(jnp.int32, (rows, LANES), 1)
    lane = lax.broadcasted_iota(jnp.int32, (own, LANES), 1)
    low = lane < head_dim

    def twice(pair, odd):
        turned = pltpu.roll(pair, head_dim, 1)
        return jnp.where(low, turned, pair) if odd else jnp.where(low, pair, turned)

    for level in range(layers):
        x = x_ref[...]
        square = jnp.sum(x * x, axis=1, keepdims=True)
        gained = (x * norm_ref[level][None, :]).astype(BF16)
        load_step(level).wait()
        extra = lax.dot_general(
            gained, w_step[level], (((1,), (1,)), ((), ())), preferred_element_type=F32)
        extra = jnp.where(lane_all == LANES - 1, square, extra).reshape(dp, own, LANES)
        high, rest = halves(extra)
        extra_send[level, :, :, :LANES] = high
        extra_send[level, :, :, LANES:] = rest
        if level == 0:
            pl.semaphore_wait(barrier, dp - 1 + tp - 1)
        each(dp - 1, lambda k: send_extra(level, k).start())
        for w in range(4):
            load_in(level, w).wait()
            part = jnp.dot(gained, w_in[level, w], preferred_element_type=F32)
            part_send[level, w] = part.reshape(dp, own, cols).astype(BF16)
            each(dp - 1, lambda k: send_part(level, w, k).start())

        if level == 0:
            step = 256

            def build(index, carry):
                start = pl.multiple_of(index * step, step)
                entry = lax.broadcasted_iota(jnp.int32, (LANES, step), 1) + start
                which = lax.broadcasted_iota(jnp.int32, (LANES, step), 0)
                spread[:, pl.ds(start, step)] = jnp.where(
                    lax.rem(which, head_dim) == entry // span, 1.0, 0.0).astype(BF16)
                entry = lax.broadcasted_iota(jnp.int32, (step, LANES), 0) + start
                which = lax.broadcasted_iota(jnp.int32, (step, LANES), 1)
                gather[pl.ds(start, step), :] = jnp.where(
                    lax.rem(which, head_dim) == entry // span, 1.0, 0.0).astype(BF16)
                return carry

            lax.fori_loop(0, head_dim * span // step, build, 0)
            pick = lax.broadcasted_iota(jnp.int32, (LANES, cols), 0)
            slot = lax.broadcasted_iota(jnp.int32, (LANES, cols), 1)
            chosen_ref[...] = jnp.where(
                pick == col * heads + slot // head_dim, 1.0, 0.0).astype(BF16)
            pick = lax.broadcasted_iota(jnp.int32, (heads, cols), 0)
            slot = lax.broadcasted_iota(jnp.int32, (heads, cols), 1)
            wider = jnp.where(pick == slot // head_dim, 1.0, 0.0)
            for place, value in enumerate((bias_ref[...], jnp.exp(rate_ref[...]), skip_ref[...])):
                params_ref[place] = jnp.dot(
                    value, wider, preferred_element_type=F32, precision=lax.Precision.HIGHEST)

        def convolve(j):
            return jnp.sum(
                recent_ref[level, :, j].astype(F32)
                * taps_ref[: taps_ref.shape[0] - 1, j, level, :].astype(F32)[None],
                axis=1,
            )

        for j in range(3):
            conv_ref[j] = convolve(j)

        each(dp - 1, lambda k: send_extra(level, k).wait_recv())

        def add_extra(k, total):
            return total + extra_recv[level, k].astype(F32)

        both = fold(dp - 1, add_extra, extra_send[level, me].astype(F32))
        total = both[:, :LANES] + both[:, LANES:]
        scale = lax.rsqrt(total[:, LANES - 1 :] / features + EPS)
        chosen = chosen_ref[...]
        high, rest = halves(total * scale)
        raw = jnp.dot(high, chosen, preferred_element_type=F32) + jnp.dot(
            rest, chosen, preferred_element_type=F32)
        raw = raw + params_ref[0, level : level + 1, :]
        size = jnp.maximum(raw, 0.0) + jnp.log1p(jnp.exp(-jnp.abs(raw)))
        decay = jnp.exp(-size * params_ref[1, level : level + 1, :])

        def total_part(w):
            each(dp - 1, lambda k: send_part(level, w, k).wait_recv())
            return scale * fold(
                dp - 1,
                lambda k, sum_in: sum_in + part_recv[level, w, k].astype(F32),
                part_send[level, w, me].astype(F32),
            )

        def active(w, place):
            u = total_part(w).astype(BF16)
            u_out[level, :, place * cols : (place + 1) * cols] = u
            return silu(
                conv_ref[place]
                + u.astype(F32) * taps_ref[taps_ref.shape[0] - 1, place, level : level + 1, :].astype(F32))

        bm = active(0, 1)
        cm = active(1, 2)
        for h in range(heads):
            window = slice(h // 2 * LANES, h // 2 * LANES + LANES)
            dec_ref[h] = twice(decay[:, window], h % 2)
            bm_ref[h] = twice(bm[:, window], h % 2)
            cm_ref[h] = twice(cm[:, window], h % 2)
        load_state(level).wait()
        piece = 512
        pieces = head_dim * span // piece

        def across(ref, h):
            return jnp.concatenate([ref[h]] * (piece // LANES), axis=1)

        def consult(index, y):
            window = pl.ds(pl.multiple_of(index * piece, piece), piece)
            read = jnp.concatenate(
                [state[level, h, :, window] * across(cm_ref, h) for h in range(heads)], axis=0)
            return y + jnp.dot(
                read.astype(BF16), gather[window, :], preferred_element_type=F32)

        y = lax.fori_loop(0, pieces, consult, jnp.zeros((heads * own, LANES), F32))
        xv = active(2, 0)
        weighted = size * xv
        inner = []
        for h in range(heads):
            window = slice(h // 2 * LANES, h // 2 * LANES + LANES)
            one = twice(weighted[:, window], h % 2)
            high = one.astype(BF16).astype(F32)
            wide_ref[h * own : (h + 1) * own, :] = jnp.where(low, high, one - high)
            within = jnp.sum(
                jnp.where(low, bm_ref[h] * cm_ref[h], 0.0), axis=1, keepdims=True)
            inner.append(dec_ref[h] * y[h * own : (h + 1) * own] + one * within)
        y = jnp.concatenate(
            [jnp.where(low, inner[h], inner[h + 1]) for h in range(0, heads, 2)], axis=1)
        y = y + params_ref[2, level : level + 1, :] * xv
        gate = total_part(3)
        gated_all[level, me] = (y * silu(gate) * gain_ref[level : level + 1, :]).astype(BF16)
        each(dp - 1, lambda k: send_gated(level, k).start())
        wide = wide_ref[...].astype(BF16)

        def advance(index, carry):
            window = pl.ds(pl.multiple_of(index * piece, piece), piece)
            grown = jnp.dot(wide, spread[:, window], preferred_element_type=F32)
            for h in range(heads):
                fresh_out[level, h, :, window] = (
                    across(dec_ref, h) * state[level, h, :, window]
                    + grown[h * own : (h + 1) * own] * across(bm_ref, h))
            return carry

        lax.fori_loop(0, pieces, advance, 0)
        load_out(level).wait()
        each(dp - 1, lambda k: send_gated(level, k).wait_recv())
        gated = gated_all[level].astype(F32).reshape(rows, cols)
        square = jnp.sum(gated * gated, axis=1, keepdims=True)
        mixed = jnp.dot(gated.astype(BF16), w_out[level], preferred_element_type=F32)
        mixed_all[level, col] = mixed.astype(BF16)
        each(tp - 1, lambda k: send_mixed(level, k).start())
        cross = lax.broadcasted_iota(jnp.int32, (rows, rows), 0) == (
            lax.broadcasted_iota(jnp.int32, (rows, rows), 1))
        square_all[level, col, :, :rows] = jnp.broadcast_to(
            jnp.sum(jnp.where(cross, square, 0.0), axis=0, keepdims=True), (8, rows))
        each(tp - 1, lambda k: send_square(level, k).start())
        each(tp - 1, lambda k: send_square(level, k).wait_recv())
        square = fold(
            tp,
            lambda k, sum_in: sum_in + square_all[level, k, 0:1, :rows],
            jnp.zeros((1, rows), F32),
        )
        scale = lax.rsqrt(square / (cols * tp) + EPS)
        scale = jnp.sum(jnp.where(cross, scale, 0.0), axis=1, keepdims=True)
        each(tp - 1, lambda k: send_mixed(level, k).wait_recv())
        mixed = fold(
            tp,
            lambda k, sum_in: sum_in + mixed_all[level, k].astype(F32),
            jnp.zeros((rows, width), F32),
        )
        fresh_x = (x_ref[...] + scale * mixed).astype(BF16)
        x_ref[...] = fresh_x.astype(F32)
        if level == layers - 1:
            tokens_out[...] = fresh_x

    for level in range(layers):
        each(dp - 1, lambda k: send_extra(level, k).wait_send())
        for w in range(4):
            each(dp - 1, lambda k: send_part(level, w, k).wait_send())
        each(dp - 1, lambda k: send_gated(level, k).wait_send())
        each(tp - 1, lambda k: send_mixed(level, k).wait_send())
        each(tp - 1, lambda k: send_square(level, k).wait_send())


def finish(
    fresh_ref, tokens_ref, u_ref, recent_ref, tokens_out, fresh_hbm, recent_out, fresh_sem
):
    layers, heads = fresh_ref.shape[:2]
    cols = recent_ref.shape[-1]

    def save(level, h):
        return pltpu.make_async_copy(
            fresh_ref.at[level, h], fresh_hbm.at[level, h], fresh_sem.at[level, h])

    for level in range(layers):
        for h in range(heads):
            save(level, h).start()
    tokens_out[...] = tokens_ref[...]
    for level in range(layers):
        for j in range(3):
            kept = recent_ref[level, :, j].astype(F32)
            u = u_ref[level, :, j * cols : (j + 1) * cols].astype(F32)
            recent_out[level, :, j] = jnp.concatenate(
                [kept[:, 1:], u[:, None]], axis=1).astype(BF16)
    for level in range(layers):
        for h in range(heads):
            save(level, h).wait()


def per_device(
    dp,
    tp,
    tokens,
    norm_gain,
    w_gate,
    w_value,
    w_inmap,
    w_readout,
    w_step,
    step_bias,
    decay_log,
    skip_gain,
    conv_taps,
    gate_gain,
    w_project,
    states,
    recent,
):
    layers, own, heads, entries = states.shape
    cols = w_gate.shape[2]
    head_dim = cols // heads
    span = entries // head_dim
    width = tokens.shape[1]
    features = width * dp
    dims = (layers, dp, tp, own, cols, heads, head_dim, span, features, width)
    rows = tokens.shape[0]

    vmem = pl.BlockSpec(memory_space=pltpu.VMEM)
    anywhere = pl.BlockSpec(memory_space=pltpu.HBM)
    turned = recent.transpose(0, 1, 3, 2, 4)
    dma = pltpu.SemaphoreType.DMA
    out_tokens, fresh, u = pl.pallas_call(
        functools.partial(kernel, dims),
        out_shape=(
            jax.ShapeDtypeStruct((rows, width), BF16),
            pltpu.VMEM((layers, heads, own, entries), F32),
            jax.ShapeDtypeStruct((layers, own, 3 * cols), BF16),
        ),
        in_specs=[vmem] * 8 + [anywhere] * 7,
        out_specs=(vmem, vmem, vmem),
        scratch_shapes=[
            pltpu.VMEM((layers, 4, width, cols), BF16),
            pltpu.VMEM((layers, LANES, width), BF16),
            pltpu.VMEM((layers, cols, width), BF16),
            pltpu.VMEM((layers, heads, own, entries), F32),
            pltpu.VMEM((LANES, entries), BF16),
            pltpu.VMEM((entries, LANES), BF16),
            pltpu.VMEM((layers, 4, dp, own, cols), BF16),
            pltpu.VMEM((layers, 4, dp - 1, own, cols), BF16),
            pltpu.VMEM((layers, dp, own, 2 * LANES), BF16),
            pltpu.VMEM((layers, dp - 1, own, 2 * LANES), BF16),
            pltpu.VMEM((layers, dp, own, cols), BF16),
            pltpu.VMEM((layers, tp, rows, width), BF16),
            pltpu.VMEM((layers, tp, 8, -(-rows // LANES) * LANES), F32),
            pltpu.VMEM((3, own, cols), F32),
            pltpu.VMEM((3, layers, cols), F32),
            pltpu.VMEM((LANES, cols), BF16),
            pltpu.VMEM((heads, own, LANES), F32),
            pltpu.VMEM((heads, own, LANES), F32),
            pltpu.VMEM((heads, own, LANES), F32),
            pltpu.VMEM((heads * own, LANES), F32),
            pltpu.VMEM((rows, width), F32),
            dma((layers, 4)),
            dma((layers,)),
            dma((layers,)),
            dma((layers,)),
            dma((layers, 4, dp - 1)),
            dma((layers, 4, dp - 1)),
            dma((layers, dp - 1)),
            dma((layers, dp - 1)),
            dma((layers, dp - 1)),
            dma((layers, dp - 1)),
            dma((layers, tp - 1)),
            dma((layers, tp - 1)),
            dma((layers, tp - 1)),
            dma((layers, tp - 1)),
        ],
        compiler_params=pltpu.CompilerParams(
            collective_id=0, has_side_effects=True, vmem_limit_bytes=56 * 1024 * 1024),
    )(
        tokens,
        norm_gain,
        step_bias,
        decay_log,
        skip_gain,
        gate_gain,
        conv_taps.transpose(1, 2, 0, 3),
        turned,
        w_value,
        w_inmap,
        w_readout,
        w_gate,
        w_step.transpose(0, 2, 1),
        w_project,
        states.transpose(0, 2, 1, 3),
    )
    out_tokens, fresh, kept = pl.pallas_call(
        finish,
        out_shape=(
            jax.ShapeDtypeStruct(out_tokens.shape, BF16),
            jax.ShapeDtypeStruct(fresh.shape, F32),
            jax.ShapeDtypeStruct(turned.shape, BF16),
        ),
        in_specs=[vmem] * 4,
        out_specs=(vmem, anywhere, vmem),
        scratch_shapes=[dma((layers, heads))],
        compiler_params=pltpu.CompilerParams(vmem_limit_bytes=16 * 1024 * 1024),
    )(fresh, out_tokens, u, turned)
    next_states = fresh.transpose(0, 2, 1, 3)
    next_recent = kept.transpose(0, 1, 3, 2, 4)
    return out_tokens, next_states, next_recent


def solution(mesh):
    in_specs = (
        P(None, "dp"),
        P(None, "dp"),
        P(None, "dp", "tp"),
        P(None, "dp", "tp"),
        P(None, "dp", "tp"),
        P(None, "dp", "tp"),
        P(None, "dp", None),
        P(None, "tp"),
        P(None, "tp"),
        P(None, "tp"),
        P(None, None, None, "tp"),
        P(None, "tp"),
        P(None, "tp", "dp"),
        P(None, "dp", "tp", None),
        P(None, "dp", None, None, "tp"),
    )
    out_specs = (P(None, "dp"), P(None, "dp", "tp", None), P(None, "dp", None, None, "tp"))
    body = functools.partial(per_device, mesh.shape["dp"], mesh.shape["tp"])
    return jax.shard_map(
        body, mesh=mesh, in_specs=in_specs, out_specs=out_specs, check_vma=False
    )
```

profile of v0, /device:TPU:0, one launch (start us, length us, event | category | flops | bytes accessed | tf_op | source)
XLA Modules:
  0.0 52.7 jit_solution(4111684131567452333)
XLA Ops:
  0.6 0.0 copy-start
  0.6 47.7 %shard_map.166 = (bf16[64,512]{1,0:T(8,128)(2,1)}, f32[2,12,8,4096]{3,2,1,0:T(8,128)S(1)}, bf16[2,8,2304]{2,1,0:T(8,128)(2,1)}) custom-call(bf16[64,512]{1,0:T(8,128)(2,1)} %tokens_ref.1, f32[2,512]{1,0:T(2,128)} %norm_ref.1, f32[2,12]{1,0:T(2,128)} %bias_ref.1, f32[2,12]{1,0:T(2,128)} %rate_ref.1, f32[2,12]{1,0:T(2,128)} %skip_ref.1, f32[2,768]{1,0:T(2,128)} %gain_ref.1, ...), custom_call_target="tpu_custom_call" | custom-call | tf_op jit(solution)/shard_map/pallas_call | solution.py:434
  48.3 0.0 copy-done
  48.4 0.0 copy-start.1
  48.4 0.9 %copy-done.1 = bf16[2,8,2304]{2,1,0:T(8,128)(2,1)S(1)} copy-done((bf16[2,8,2304]{2,1,0:T(8,128)(2,1)S(1)}, bf16[2,8,2304]{2,1,0:T(8,128)(2,1)}, u32[]{:S(2)}) %copy-start.1) | copy-done | bytes 73752
  49.2 0.0 copy-start.2
  49.2 0.8 %copy-done.2 = bf16[64,512]{1,0:T(8,128)(2,1)S(1)} copy-done((bf16[64,512]{1,0:T(8,128)(2,1)S(1)}, bf16[64,512]{1,0:T(8,128)(2,1)}, u32[]{:S(2)}) %copy-start.2) | copy-done | bytes 65560
  50.1 2.6 %shard_map.167 = (bf16[64,512]{1,0:T(8,128)(2,1)}, f32[2,12,8,4096]{3,2,1,0:T(8,128)}, bf16[2,8,3,4,768]{4,3,2,1,0:T(4,128)(2,1)}) custom-call(f32[2,12,8,4096]{3,2,1,0:T(8,128)S(1)} %get-tuple-element.9.fresh_ref, bf16[64,512]{1,0:T(8,128)(2,1)S(1)} %copy-done.2, bf16[2,8,2304]{2,1,0:T(8,128)(2,1)S(1)} %copy-done.1, bf16[2,8,3,4,768]{4,3,2,1,0:T(4,128)(2,1)S(1)} %bitcast.7), custom_call_target="tpu_custom_call" | custom-call | tf_op jit(solution)/shard_map/pallas_call | solution.py:499
Async XLA Ops:
  0.6 47.7 %copy-start = (bf16[2,8,4,3,768]{4,2,3,1,0:T(4,128)(2,1)S(1)}, bf16[2,8,4,3,768]{4,2,3,1,0:T(4,128)(2,1)}, u32[]{:S(2)}) copy-start(bf16[2,8,4,3,768]{4,2,3,1,0:T(4,128)(2,1)} %param.29) | copy-start | bytes 884740
  48.4 0.9 %copy-start.1 = (bf16[2,8,2304]{2,1,0:T(8,128)(2,1)S(1)}, bf16[2,8,2304]{2,1,0:T(8,128)(2,1)}, u32[]{:S(2)}) copy-start(bf16[2,8,2304]{2,1,0:T(8,128)(2,1)} %get-tuple-element.11.u_ref) | copy-start | bytes 221188
  49.2 0.8 %copy-start.2 = (bf16[64,512]{1,0:T(8,128)(2,1)S(1)}, bf16[64,512]{1,0:T(8,128)(2,1)}, u32[]{:S(2)}) copy-start(bf16[64,512]{1,0:T(8,128)(2,1)} %get-tuple-element.10.tokens_ref) | copy-start | bytes 196612
where the time goes:
time: 52.9 us; the launch traced here: 52.7 us
  Pallas kernels  50.3 us (95%)
  local copies, waits for them, and re-layouts  1.72 us (3%)
  between operations  0.67 us (1%)
    pallas_call x1, Pallas kernels, per_device(): pl.pallas_call(functools.partial(kernel, dims), out_shape=(jax.ShapeDtype...  47.7 us
    pallas_call x1, Pallas kernels, per_device(): pl.pallas_call(finish, out_shape=(jax.ShapeDtypeStruct(out_tokens.shape,...  2.58 us
    unnamed x6, local copies, waits for them, and re-layouts  1.72 us

commit v1 on v0

v1 whole, which is shorter than its diff:
```python
import functools

import jax
import jax.numpy as jnp
from jax import lax
from jax.experimental import pallas as pl
from jax.experimental.pallas import tpu as pltpu
from jax.sharding import PartitionSpec as P

EPS = 1e-06
LANES = 128
MESH = pl.DeviceIdType.MESH
F32 = jnp.float32
BF16 = jnp.bfloat16
VMEM_BYTES = 67043328
READOUT, INMAP, VALUE, GATE = range(4)


def each(count, body, first=0):
    if count - first <= 8:
        for index in range(first, count):
            body(index)
    else:
        lax.fori_loop(first, count, lambda index, carry: (body(index), carry)[1], 0)


def fold(count, body, start, first=0):
    if count - first <= 8:
        for index in range(first, count):
            start = body(index, start)
        return start
    return lax.fori_loop(first, count, body, start)


def silu(value):
    return value / (1.0 + jnp.exp(-value))


def halves(value):
    high = value.astype(BF16)
    return high, (value - high.astype(F32)).astype(BF16)


def kernel(
    dims,
    tokens_hbm,
    norm_hbm,
    bias_hbm,
    rate_hbm,
    skip_hbm,
    gain_hbm,
    taps_hbm,
    recent_hbm,
    readout_hbm,
    inmap_hbm,
    value_hbm,
    gate_hbm,
    step_hbm,
    project_hbm,
    states_hbm,
    tokens_out,
    fresh_out,
    recent_out,
    tokens_ref,
    norm_ref,
    bias_ref,
    rate_ref,
    skip_ref,
    gain_ref,
    taps_ref,
    recent_ref,
    w_in,
    w_step,
    w_out,
    state,
    spread,
    gather,
    part_send,
    part_recv,
    extra_send,
    extra_recv,
    gated_all,
    mixed_all,
    square_all,
    conv_ref,
    params_ref,
    chosen_ref,
    dec_ref,
    bm_ref,
    cm_ref,
    wide_ref,
    x_ref,
    small_sem,
    in_sem,
    step_sem,
    out_sem,
    state_sem,
    send_sem,
    extra_sem,
    part_sem,
    gated_sem,
    mixed_sem,
    square_sem,
):
    layers, groups, dp, tp, own, cols, heads, head_dim, span, features, width = dims
    me = lax.axis_index("dp")
    col = lax.axis_index("tp")
    members = dp // groups
    rows = members * own
    mine = me // members
    place = lax.rem(me, members)

    def source(k):
        return lax.rem(me + k, dp)

    def member(g, k):
        return g * members + lax.rem(place + k, members)

    def column(k):
        return lax.rem(col + k + 1, tp)

    small = [
        pltpu.make_async_copy(far, near, small_sem.at[index])
        for index, (far, near) in enumerate((
            (tokens_hbm, tokens_ref),
            (norm_hbm, norm_ref),
            (bias_hbm, bias_ref),
            (rate_hbm, rate_ref),
            (skip_hbm, skip_ref),
            (gain_hbm, gain_ref),
            (taps_hbm, taps_ref),
            (recent_hbm, recent_ref),
        ))
    ]
    sources = (readout_hbm, inmap_hbm, value_hbm, gate_hbm)
    filled = step_hbm.shape[1]

    def load_step(level):
        return pltpu.make_async_copy(
            step_hbm.at[level], w_step.at[level, :filled], step_sem.at[level])

    def load_in(level, w):
        return pltpu.make_async_copy(
            sources[w].at[level], w_in.at[level, w], in_sem.at[level, w])

    def load_out(level):
        return pltpu.make_async_copy(project_hbm.at[level], w_out.at[level], out_sem.at[level])

    def load_state(level):
        return pltpu.make_async_copy(states_hbm.at[level], state.at[level], state_sem.at[level])

    for copy in small:
        copy.start()
    load_step(0).start()
    for w in range(4):
        load_in(0, w).start()

    barrier = pltpu.get_barrier_semaphore()
    each(dp, lambda k: pl.semaphore_signal(
        barrier, inc=1, device_id={"dp": source(k)}, device_id_type=MESH), 1)
    each(tp - 1, lambda k: pl.semaphore_signal(
        barrier, inc=1, device_id={"tp": column(k)}, device_id_type=MESH))

    def slot(target, origin):
        return lax.rem(origin - target + dp, dp) - 1

    def send_extra(level, target, origin):
        return pltpu.make_async_remote_copy(
            src_ref=extra_send.at[level, target],
            dst_ref=extra_recv.at[level, slot(target, origin)],
            send_sem=send_sem.at[0],
            recv_sem=extra_sem.at[level],
            device_id={"dp": target},
            device_id_type=MESH,
        )

    def send_part(level, w, target, origin):
        return pltpu.make_async_remote_copy(
            src_ref=part_send.at[level, w, target],
            dst_ref=part_recv.at[level, w, slot(target, origin)],
            send_sem=send_sem.at[1],
            recv_sem=part_sem.at[level, w],
            device_id={"dp": target},
            device_id_type=MESH,
        )

    def send_gated(level, target, origin):
        return pltpu.make_async_remote_copy(
            src_ref=gated_all.at[level, origin],
            dst_ref=gated_all.at[level, origin],
            send_sem=send_sem.at[2],
            recv_sem=gated_sem.at[level, mine],
            device_id={"dp": target},
            device_id_type=MESH,
        )

    def send_mixed(level, g, target, origin):
        return pltpu.make_async_remote_copy(
            src_ref=mixed_all.at[level, g, origin],
            dst_ref=mixed_all.at[level, g, origin],
            send_sem=send_sem.at[3],
            recv_sem=mixed_sem.at[level, g],
            device_id={"tp": target},
            device_id_type=MESH,
        )

    def send_square(level, g, target, origin):
        return pltpu.make_async_remote_copy(
            src_ref=square_all.at[level, g, origin],
            dst_ref=square_all.at[level, g, origin],
            send_sem=send_sem.at[4],
            recv_sem=square_sem.at[level, g],
            device_id={"tp": target},
            device_id_type=MESH,
        )

    def arrived(ref, sem):
        pltpu.make_async_remote_copy(
            src_ref=ref,
            dst_ref=ref,
            send_sem=send_sem.at[0],
            recv_sem=sem,
            device_id={"dp": source(1)},
            device_id_type=MESH,
        ).wait_recv()

    def sent(ref, index):
        pltpu.make_async_remote_copy(
            src_ref=ref,
            dst_ref=ref,
            send_sem=send_sem.at[index],
            recv_sem=extra_sem.at[0],
            device_id={"dp": source(1)},
            device_id_type=MESH,
        ).wait_send()

    def others(g, body):
        each(members, lambda k: body(member(g, k)), 1)
        if groups > 1:
            pl.when(mine != g)(lambda: body(member(g, 0)))

    low = lax.broadcasted_iota(jnp.int32, (own, LANES), 1) < head_dim

    def twice(pair, odd):
        turned = pltpu.roll(pair, head_dim, 1)
        return jnp.where(low, turned, pair) if odd else jnp.where(low, pair, turned)

    def project_in(level, first, count):
        span_rows = slice(first * rows, (first + count) * rows)
        span_devices = slice(first * members, (first + count) * members)
        x = x_ref[span_rows]
        square = jnp.sum(x * x, axis=1, keepdims=True)
        gained = (x * norm_ref[level][None, :]).astype(BF16)
        lane = lax.broadcasted_iota(jnp.int32, (count * rows, LANES), 1)
        load_step(level).wait() if first == 0 else None
        extra = lax.dot_general(
            gained, w_step[level], (((1,), (1,)), ((), ())), preferred_element_type=F32)
        extra = jnp.where(lane == LANES - 1, square, extra).reshape(count * members, own, LANES)
        high, rest = halves(extra)
        extra_send[level, span_devices, :, :LANES] = high
        extra_send[level, span_devices, :, LANES:] = rest
        if level == 0 and first == 0:
            pl.semaphore_wait(barrier, dp - 1 + tp - 1)
        others(first, lambda target: send_extra(level, target, me).start())
        for w in range(4):
            if first == 0:
                with jax.named_scope(f"w_in{w}_{level}"):
                    load_in(level, w).wait()
            part = jnp.dot(gained, w_in[level, w], preferred_element_type=F32)
            part_send[level, w, span_devices] = part.reshape(
                count * members, own, cols).astype(BF16)
            with jax.named_scope(f"send{w}_{level}_{first}"):
                others(first, lambda target: send_part(level, w, target, me).start())
        for g in range(first + 1, first + count):
            others(g, lambda target: send_extra(level, target, me).start())
            for w in range(4):
                others(g, lambda target: send_part(level, w, target, me).start())

    def prepare():
        w_step[:, filled:] = jnp.zeros((layers, LANES - filled, width), BF16)

    def build():
        step = 256
        which = lax.broadcasted_iota(jnp.int32, (LANES, step), 0)
        entry = lax.broadcasted_iota(jnp.int32, (LANES, step), 1)
        across_lanes = lax.rem(which, head_dim) - entry // span
        which = lax.broadcasted_iota(jnp.int32, (step, LANES), 1)
        entry = lax.broadcasted_iota(jnp.int32, (step, LANES), 0)
        along_rows = lax.rem(which, head_dim) - entry // span

        def fill(index, carry):
            start = pl.multiple_of(index * step, step)
            target = index * (step // span)
            spread[:, pl.ds(start, step)] = jnp.where(
                across_lanes == target, 1.0, 0.0).astype(BF16)
            gather[pl.ds(start, step), :] = jnp.where(
                along_rows == target, 1.0, 0.0).astype(BF16)
            return carry

        lax.fori_loop(0, head_dim * span // step, fill, 0)
        pick = lax.broadcasted_iota(jnp.int32, (LANES, cols), 0)
        slot = lax.broadcasted_iota(jnp.int32, (LANES, cols), 1)
        chosen_ref[...] = jnp.where(
            pick == col * heads + slot // head_dim, 1.0, 0.0).astype(BF16)
        pick = lax.broadcasted_iota(jnp.int32, (heads, cols), 0)
        slot = lax.broadcasted_iota(jnp.int32, (heads, cols), 1)
        wider = jnp.where(pick == slot // head_dim, 1.0, 0.0)
        for where, value in enumerate((bias_ref[...], jnp.exp(rate_ref[...]), skip_ref[...])):
            params_ref[where] = jnp.dot(
                value, wider, preferred_element_type=F32, precision=lax.Precision.HIGHEST)

    def convolve(level):
        for j in range(3):
            conv_ref[level, j] = jnp.sum(
                recent_ref[level, :, j].astype(F32)
                * taps_ref[: taps_ref.shape[0] - 1, j, level, :].astype(F32)[None],
                axis=1,
            )

    piece = 1024
    pieces = head_dim * span // piece

    def across(ref, h):
        return jnp.concatenate([ref[h]] * (piece // LANES), axis=1)

    def mix(level):
        with jax.named_scope(f"wr_extra_{level}"):
            arrived(extra_recv.at[level], extra_sem.at[level])
        both = fold(
            dp - 1,
            lambda k, sum_in: sum_in + extra_recv[level, k].astype(F32),
            extra_send[level, me].astype(F32),
        )
        total = both[:, :LANES] + both[:, LANES:]
        scale = lax.rsqrt(total[:, LANES - 1 :] / features + EPS)
        chosen = chosen_ref[...]
        high, rest = halves(total * scale)
        raw = jnp.dot(high, chosen, preferred_element_type=F32) + jnp.dot(
            rest, chosen, preferred_element_type=F32)
        raw = raw + params_ref[0, level : level + 1, :]
        size = jnp.maximum(raw, 0.0) + jnp.log1p(jnp.exp(-jnp.abs(raw)))
        decay = jnp.exp(-size * params_ref[1, level : level + 1, :])

        def total_part(w):
            with jax.named_scope(f"wr_part{w}_{level}"):
                arrived(part_recv.at[level, w], part_sem.at[level, w])
            return scale * fold(
                dp - 1,
                lambda k, sum_in: sum_in + part_recv[level, w, k].astype(F32),
                part_send[level, w, me].astype(F32),
            )

        fresh_u = {}

        def active(w, j):
            u = total_part(w).astype(BF16).astype(F32)
            fresh_u[j] = u
            return silu(
                conv_ref[level, j]
                + u * taps_ref[taps_ref.shape[0] - 1, j, level : level + 1, :].astype(F32))

        cm = active(READOUT, 2)
        for h in range(heads):
            window = slice(h // 2 * LANES, h // 2 * LANES + LANES)
            cm_ref[h] = twice(cm[:, window], h % 2)
        with jax.named_scope(f"w_state_{level}"):
            load_state(level).wait()
        y = jnp.zeros((heads * own, LANES), F32)
        with jax.named_scope(f"consult_{level}"):
            for index in range(pieces):
                window = slice(index * piece, index * piece + piece)
                read = jnp.concatenate(
                    [state[level, h, :, window] * across(cm_ref, h) for h in range(heads)], axis=0)
                y = y + jnp.dot(
                    read.astype(BF16), gather[window, :], preferred_element_type=F32)
        bm = active(INMAP, 1)
        for h in range(heads):
            window = slice(h // 2 * LANES, h // 2 * LANES + LANES)
            dec_ref[h] = twice(decay[:, window], h % 2)
            bm_ref[h] = twice(bm[:, window], h % 2)
        xv = active(VALUE, 0)
        weighted = size * xv
        inner = []
        for h in range(heads):
            window = slice(h // 2 * LANES, h // 2 * LANES + LANES)
            one = twice(weighted[:, window], h % 2)
            high = one.astype(BF16).astype(F32)
            wide_ref[h * own : (h + 1) * own, :] = jnp.where(low, high, one - high)
            within = jnp.sum(
                jnp.where(low, bm_ref[h] * cm_ref[h], 0.0), axis=1, keepdims=True)
            inner.append(dec_ref[h] * y[h * own : (h + 1) * own] + one * within)
        y = jnp.concatenate(
            [jnp.where(low, inner[h], inner[h + 1]) for h in range(0, heads, 2)], axis=1)
        y = (y + params_ref[2, level : level + 1, :] * xv) * gain_ref[level : level + 1, :]
        gate = total_part(GATE)
        gated_all[level, me] = (y * silu(gate)).astype(BF16)
        with jax.named_scope(f"s_gated_{level}"):
            each(dp, lambda k: send_gated(level, source(k), me).start(), 1)
        with jax.named_scope(f"advance_{level}"):
            wide = wide_ref[...].astype(BF16)

            def advance(index, carry):
                window = pl.ds(pl.multiple_of(index * piece, piece), piece)
                grown = jnp.dot(wide, spread[:, window], preferred_element_type=F32)
                for h in range(heads):
                    fresh_out[level, h, :, window] = (
                        across(dec_ref, h) * state[level, h, :, window]
                        + grown[h * own : (h + 1) * own] * across(bm_ref, h))
                return carry

            lax.fori_loop(0, pieces, advance, 0)
        with jax.named_scope(f"recent_{level}"):
            for j in range(3):
                kept = recent_ref[level, :, j].astype(F32)
                recent_out[level, :, j] = jnp.concatenate(
                    [kept[:, 1:], fresh_u[j][:, None]], axis=1).astype(BF16)

    cross = lax.broadcasted_iota(jnp.int32, (rows, rows), 0) == (
        lax.broadcasted_iota(jnp.int32, (rows, rows), 1))

    def project_out(level, g):
        if g == 0:
            load_out(level).wait()
        with jax.named_scope(f"wr_gated_{level}_{g}"):
            sem = gated_sem.at[level, g]
            if groups > 1:
                pl.when(mine == g)(lambda: arrived(gated_all.at[level, : members - 1], sem))
                pl.when(mine != g)(lambda: arrived(gated_all.at[level, :members], sem))
            else:
                arrived(gated_all.at[level, : members - 1], sem)
        gated = gated_all[level, g * members : (g + 1) * members].astype(F32).reshape(rows, cols)
        square = jnp.sum(gated * gated, axis=1, keepdims=True)
        square_all[level, g, col, :, :rows] = jnp.sum(
            jnp.where(cross, square, 0.0), axis=0, keepdims=True)
        each(tp - 1, lambda k: send_square(level, g, column(k), col).start())
        mixed = jnp.dot(gated.astype(BF16), w_out[level], preferred_element_type=F32)
        mixed_all[level, g, col] = mixed.astype(BF16)
        with jax.named_scope(f"s_mixed_{level}_{g}"):
            each(tp - 1, lambda k: send_mixed(level, g, column(k), col).start())

    def renew(level, g):
        arrived(square_all.at[level, g, : tp - 1], square_sem.at[level, g])
        square = fold(
            tp,
            lambda k, sum_in: sum_in + square_all[level, g, k, :, :rows],
            jnp.zeros((1, rows), F32),
        )
        scale = lax.rsqrt(square / (cols * tp) + EPS)
        scale = jnp.sum(jnp.where(cross, scale, 0.0), axis=1, keepdims=True)
        with jax.named_scope(f"wr_mixed_{level}_{g}"):
            arrived(mixed_all.at[level, g, : tp - 1], mixed_sem.at[level, g])
        mixed = fold(
            tp,
            lambda k, sum_in: sum_in + mixed_all[level, g, k].astype(F32),
            jnp.zeros((rows, width), F32),
        )
        window = slice(g * rows, (g + 1) * rows)
        fresh_x = (x_ref[window] + scale * mixed).astype(BF16)
        if level == layers - 1:
            tokens_out[window] = fresh_x
        else:
            x_ref[window] = fresh_x.astype(F32)

    prepare()
    small[0].wait()
    small[1].wait()
    x_ref[...] = tokens_ref[...].astype(F32)
    project_in(0, 0, groups)
    load_state(0).start()
    load_out(0).start()
    for level in range(1, layers):
        load_step(level).start()
        for w in range(4):
            load_in(level, w).start()
        load_state(level).start()
        load_out(level).start()
    with jax.named_scope("small_wait"):
        for copy in small[2:]:
            copy.wait()
    with jax.named_scope("build"):
        build()
        for level in range(layers):
            convolve(level)
    for level in range(layers):
        mix(level)
        for g in range(groups):
            project_out(level, g)
        for g in range(groups):
            renew(level, g)
            if level < layers - 1:
                project_in(level + 1, g, 1)

    sent(extra_recv, 0)
    sent(part_recv, 1)
    sent(part_recv.at[:, 0], 2)
    sent(mixed_all.at[:, :, : tp - 1], 3)
    sent(square_all.at[:, :, : tp - 1], 4)


def finish(tokens_ref, fresh_ref, recent_ref, tokens_hbm, fresh_hbm, recent_hbm, sem):
    layers, heads = fresh_ref.shape[:2]
    for level in range(layers):
        for h in range(heads):
            pltpu.make_async_copy(
                fresh_ref.at[level, h], fresh_hbm.at[level, h], sem.at[0]).start()
    small = (
        pltpu.make_async_copy(tokens_ref, tokens_hbm, sem.at[1]),
        pltpu.make_async_copy(recent_ref, recent_hbm, sem.at[2]),
    )
    for copy in small:
        copy.start()
    for copy in small:
        copy.wait()
    pltpu.make_async_copy(fresh_ref, fresh_hbm, sem.at[0]).wait()


def per_device(
    dp,
    tp,
    tokens,
    norm_gain,
    w_gate,
    w_value,
    w_inmap,
    w_readout,
    w_step,
    step_bias,
    decay_log,
    skip_gain,
    conv_taps,
    gate_gain,
    w_project,
    states,
    recent,
):
    layers, own, heads, entries = states.shape
    cols = w_gate.shape[2]
    head_dim = cols // heads
    span = entries // head_dim
    width = tokens.shape[1]
    features = width * dp
    groups = GROUPS if dp % GROUPS == 0 else 1
    dims = (layers, groups, dp, tp, own, cols, heads, head_dim, span, features, width)
    total = tokens.shape[0]
    rows = total // groups

    vmem = pl.BlockSpec(memory_space=pltpu.VMEM)
    anywhere = pl.BlockSpec(memory_space=pltpu.HBM)
    turned = recent.transpose(0, 1, 3, 2, 4)
    taps = conv_taps.transpose(1, 2, 0, 3)
    dma = pltpu.SemaphoreType.DMA
    padded = -(-rows // LANES) * LANES
    kept_bytes = 2 * tokens.size + 4 * states.size + 2 * recent.size
    results = pl.pallas_call(
        functools.partial(kernel, dims),
        out_shape=(
            pltpu.VMEM((total, width), BF16),
            pltpu.VMEM((layers, heads, own, entries), F32),
            pltpu.VMEM(turned.shape, BF16),
        ),
        in_specs=[anywhere] * 15,
        out_specs=(vmem, vmem, vmem),
        scratch_shapes=[
            pltpu.VMEM(tokens.shape, BF16),
            pltpu.VMEM(norm_gain.shape, F32),
            pltpu.VMEM(step_bias.shape, F32),
            pltpu.VMEM(decay_log.shape, F32),
            pltpu.VMEM(skip_gain.shape, F32),
            pltpu.VMEM(gate_gain.shape, F32),
            pltpu.VMEM(taps.shape, BF16),
            pltpu.VMEM(turned.shape, BF16),
            pltpu.VMEM((layers, 4, width, cols), BF16),
            pltpu.VMEM((layers, LANES, width), BF16),
            pltpu.VMEM((layers, cols, width), BF16),
            pltpu.VMEM((layers, heads, own, entries), F32),
            pltpu.VMEM((LANES, entries), BF16),
            pltpu.VMEM((entries, LANES), BF16),
            pltpu.VMEM((layers, 4, dp, own, cols), BF16),
            pltpu.VMEM((layers, 4, dp - 1, own, cols), BF16),
            pltpu.VMEM((layers, dp, own, 2 * LANES), BF16),
            pltpu.VMEM((layers, dp - 1, own, 2 * LANES), BF16),
            pltpu.VMEM((layers, dp, own, cols), BF16),
            pltpu.VMEM((layers, groups, tp, rows, width), BF16),
            pltpu.VMEM((layers, groups, tp, 1, padded), F32),
            pltpu.VMEM((layers, 3, own, cols), F32),
            pltpu.VMEM((3, layers, cols), F32),
            pltpu.VMEM((LANES, cols), BF16),
            pltpu.VMEM((heads, own, LANES), F32),
            pltpu.VMEM((heads, own, LANES), F32),
            pltpu.VMEM((heads, own, LANES), F32),
            pltpu.VMEM((heads * own, LANES), F32),
            pltpu.VMEM((total, width), F32),
            dma((8,)),
            dma((layers, 4)),
            dma((layers,)),
            dma((layers,)),
            dma((layers,)),
            dma((5,)),
            dma((layers,)),
            dma((layers, 4)),
            dma((layers, groups)),
            dma((layers, groups)),
            dma((layers, groups)),
        ],
        compiler_params=pltpu.CompilerParams(
            collective_id=0, has_side_effects=True, vmem_limit_bytes=VMEM_BYTES - kept_bytes),
    )(
        tokens,
        norm_gain,
        step_bias,
        decay_log,
        skip_gain,
        gate_gain,
        taps,
        turned,
        w_readout,
        w_inmap,
        w_value,
        w_gate,
        w_step.transpose(0, 2, 1),
        w_project,
        states.transpose(0, 2, 1, 3),
    )
    out_tokens, fresh, kept = pl.pallas_call(
        finish,
        out_shape=(
            jax.ShapeDtypeStruct((total, width), BF16),
            jax.ShapeDtypeStruct((layers, heads, own, entries), F32),
            jax.ShapeDtypeStruct(turned.shape, BF16),
        ),
        in_specs=[vmem] * 3,
        out_specs=(anywhere,) * 3,
        scratch_shapes=[dma((3,))],
        compiler_params=pltpu.CompilerParams(vmem_limit_bytes=16 * 1024 * 1024),
    )(*results)
    next_states = fresh.transpose(0, 2, 1, 3)
    next_recent = kept.transpose(0, 1, 3, 2, 4)
    return out_tokens, next_states, next_recent


GROUPS = 2
def solution(mesh):
    in_specs = (
        P(None, "dp"),
        P(None, "dp"),
        P(None, "dp", "tp"),
        P(None, "dp", "tp"),
        P(None, "dp", "tp"),
        P(None, "dp", "tp"),
        P(None, "dp", None),
        P(None, "tp"),
        P(None, "tp"),
        P(None, "tp"),
        P(None, None, None, "tp"),
        P(None, "tp"),
        P(None, "tp", "dp"),
        P(None, "dp", "tp", None),
        P(None, "dp", None, None, "tp"),
    )
    out_specs = (P(None, "dp"), P(None, "dp", "tp", None), P(None, "dp", None, None, "tp"))
    body = functools.partial(per_device, mesh.shape["dp"], mesh.shape["tp"])
    return jax.shard_map(
        body, mesh=mesh, in_specs=in_specs, out_specs=out_specs, check_vma=False
    )
```

time: 52.9 us -> 41 us (0.78)
  Pallas kernels: 50.3 us -> 40.2 us
  local copies, waits for them, and re-layouts: 1.72 us -> 0 us
    pallas_call x2, Pallas kernels: 50.3 us -> 40.2 us  [the longest x1 38.4 us: per_device(): pl.pallas_call(functools.partial(kernel, dims), out_shape=(pltpu.VMEM((to...]
    unnamed x6 -> x0, local copies, waits for them, and re-layouts: 1.72 us -> none
where the time goes in v1:
time: 41 us; the launch traced here: 40.9 us
  Pallas kernels  40.2 us (98%)
  between operations  0.64 us (2%)
    pallas_call x1, Pallas kernels, per_device(): pl.pallas_call(functools.partial(kernel, dims), out_shape=(pltpu.VMEM((to...  38.4 us
    pallas_call x1, Pallas kernels, per_device(): pl.pallas_call(finish, out_shape=(jax.ShapeDtypeStruct((total, width), BF...  1.79 us

profile of v1, /device:TPU:0, one launch (start us, length us, event | category | flops | bytes accessed | tf_op | source)
XLA Modules:
  0.0 40.9 jit_solution(17678704121375044637)
XLA Ops:
  0.6 38.4 %shard_map.166 = (bf16[64,512]{1,0:T(8,128)(2,1)S(1)}, f32[2,12,8,4096]{3,2,1,0:T(8,128)S(1)}, bf16[2,8,3,4,768]{4,3,2,1,0:T(4,128)(2,1)S(1)}) custom-call(bf16[64,512]{1,0:T(8,128)(2,1)} %tokens_hbm.1, f32[2,512]{1,0:T(2,128)} %norm_hbm.1, f32[2,12]{1,0:T(2,128)} %bias_hbm.1, f32[2,12]{1,0:T(2,128)} %rate_hbm.1, f32[2,12]{1,0:T(2,128)} %skip_hbm.1, ...), custom_call_target="tpu_custom_call" | custom-call | tf_op jit(solution)/shard_map/pallas_call | solution.py:554
  39.1 1.8 %shard_map.167 = (bf16[64,512]{1,0:T(8,128)(2,1)}, f32[2,12,8,4096]{3,2,1,0:T(8,128)}, bf16[2,8,3,4,768]{4,3,2,1,0:T(4,128)(2,1)}) custom-call(bf16[64,512]{1,0:T(8,128)(2,1)S(1)} %get-tuple-element.9.tokens_ref, f32[2,12,8,4096]{3,2,1,0:T(8,128)S(1)} %get-tuple-element.10.fresh_ref, bf16[2,8,3,4,768]{4,3,2,1,0:T(4,128)(2,1)S(1)} %get-tuple-element.11.recent_ref), custom_call_target="tpu_custom_call" | custom-call | tf_op jit(solution)/shard_map/pallas_call | solution.py:624

commit v2 on v1

--- a/solution.py
+++ b/solution.py
@@ -107,17 +107,31 @@
     col = lax.axis_index("tp")
     members = dp // groups
     rows = members * own
-    mine = me // members
-    place = lax.rem(me, members)
-
-    def source(k):
-        return lax.rem(me + k, dp)
+    mine = lax.rem(me, groups)
+    place = me // groups
+
+    def moved(k):
+        if members & (members - 1):
+            return lax.rem(place + k, members)
+        return sum(
+            lax.rem(place // bit + k // bit, 2) * bit
+            for bit in (1 << power for power in range(members.bit_length() - 1)))
 
     def member(g, k):
-        return g * members + lax.rem(place + k, members)
+        return moved(k) * groups + g
+
+    def slot(g, k):
+        return k * groups + lax.rem(g - mine + groups, groups) - 1
 
     def column(k):
         return lax.rem(col + k + 1, tp)
+
+    def columns(body):
+        def at(index):
+            pl.when(col + tp - index < tp)(lambda: body(col + tp - index))
+            pl.when(col + index >= tp)(lambda: body(col + index - tp))
+
+        each(tp, at, 1)
 
     small = [
         pltpu.make_async_copy(far, near, small_sem.at[index])
@@ -149,48 +163,45 @@
     def load_state(level):
         return pltpu.make_async_copy(states_hbm.at[level], state.at[level], state_sem.at[level])
 
-    for copy in small:
+    for copy in small[:2]:
         copy.start()
     load_step(0).start()
-    for w in range(4):
-        load_in(0, w).start()
+    load_in(0, 0).start()
+    load_in(0, 1).start()
 
     barrier = pltpu.get_barrier_semaphore()
     each(dp, lambda k: pl.semaphore_signal(
-        barrier, inc=1, device_id={"dp": source(k)}, device_id_type=MESH), 1)
+        barrier, inc=1, device_id={"dp": lax.rem(me + k, dp)}, device_id_type=MESH), 1)
     each(tp - 1, lambda k: pl.semaphore_signal(
         barrier, inc=1, device_id={"tp": column(k)}, device_id_type=MESH))
 
-    def slot(target, origin):
-        return lax.rem(origin - target + dp, dp) - 1
-
-    def send_extra(level, target, origin):
+    def send_extra(level, g, k):
         return pltpu.make_async_remote_copy(
-            src_ref=extra_send.at[level, target],
-            dst_ref=extra_recv.at[level, slot(target, origin)],
+            src_ref=extra_send.at[level, g, moved(k)],
+            dst_ref=extra_recv.at[level, slot(g, k)],
             send_sem=send_sem.at[0],
             recv_sem=extra_sem.at[level],
-            device_id={"dp": target},
+            device_id={"dp": member(g, k)},
             device_id_type=MESH,
         )
 
-    def send_part(level, w, target, origin):
+    def send_part(level, w, g, k):
         return pltpu.make_async_remote_copy(
-            src_ref=part_send.at[level, w, target],
-            dst_ref=part_recv.at[level, w, slot(target, origin)],
+            src_ref=part_send.at[level, w, g, moved(k)],
+            dst_ref=part_recv.at[level, w, slot(g, k)],
             send_sem=send_sem.at[1],
             recv_sem=part_sem.at[level, w],
-            device_id={"dp": target},
+            device_id={"dp": member(g, k)},
             device_id_type=MESH,
         )
 
-    def send_gated(level, target, origin):
+    def send_gated(level, g, k):
         return pltpu.make_async_remote_copy(
-            src_ref=gated_all.at[level, origin],
-            dst_ref=gated_all.at[level, origin],
+            src_ref=gated_all.at[level, mine, place],
+            dst_ref=gated_all.at[level, mine, place],
             send_sem=send_sem.at[2],
             recv_sem=gated_sem.at[level, mine],
-            device_id={"dp": target},
+            device_id={"dp": member(g, k)},
             device_id_type=MESH,
         )
 
@@ -220,7 +231,7 @@
             dst_ref=ref,
             send_sem=send_sem.at[0],
             recv_sem=sem,
-            device_id={"dp": source(1)},
+            device_id={"dp": lax.rem(me + 1, dp)},
             device_id_type=MESH,
         ).wait_recv()
 
@@ -230,14 +241,22 @@
             dst_ref=ref,
             send_sem=send_sem.at[index],
             recv_sem=extra_sem.at[0],
-            device_id={"dp": source(1)},
+            device_id={"dp": lax.rem(me + 1, dp)},
             device_id_type=MESH,
         ).wait_send()
 
-    def others(g, body):
-        each(members, lambda k: body(member(g, k)), 1)
-        if groups > 1:
-            pl.when(mine != g)(lambda: body(member(g, 0)))
+    def others(which, body):
+        def far(index):
+            for g in which:
+                body(g, members - index)
+
+        each(members, far, 1)
+        for g in which:
+            if groups > 1:
+                pl.when(mine != g)(functools.partial(body, g, 0))
+
+    def every(level, w, which):
+        others(which, lambda g, k: send_part(level, w, g, k).start())
 
     low = lax.broadcasted_iota(jnp.int32, (own, LANES), 1) < head_dim
 
@@ -246,35 +265,45 @@
         return jnp.where(low, turned, pair) if odd else jnp.where(low, pair, turned)
 
     def project_in(level, first, count):
-        span_rows = slice(first * rows, (first + count) * rows)
-        span_devices = slice(first * members, (first + count) * members)
-        x = x_ref[span_rows]
+        x = x_ref[first : first + count].reshape(count * rows, width)
         square = jnp.sum(x * x, axis=1, keepdims=True)
         gained = (x * norm_ref[level][None, :]).astype(BF16)
         lane = lax.broadcasted_iota(jnp.int32, (count * rows, LANES), 1)
-        load_step(level).wait() if first == 0 else None
+
+        def store(w):
+            part = jnp.dot(gained, w_in[level, w], preferred_element_type=F32)
+            part_send[level, w, first : first + count] = part.reshape(
+                count, members, own, cols).astype(BF16)
+
+        if first == 0:
+            with jax.named_scope(f"w_step_{level}"):
+                load_step(level).wait()
         extra = lax.dot_general(
             gained, w_step[level], (((1,), (1,)), ((), ())), preferred_element_type=F32)
-        extra = jnp.where(lane == LANES - 1, square, extra).reshape(count * members, own, LANES)
+        extra = jnp.where(lane == LANES - 1, square, extra).reshape(count, members, own, LANES)
         high, rest = halves(extra)
-        extra_send[level, span_devices, :, :LANES] = high
-        extra_send[level, span_devices, :, LANES:] = rest
+        if first == 0:
+            with jax.named_scope(f"w_in0_{level}"):
+                load_in(level, 0).wait()
+        extra_send[level, first : first + count, :, :, :LANES] = high
+        extra_send[level, first : first + count, :, :, LANES:] = rest
+        store(0)
         if level == 0 and first == 0:
-            pl.semaphore_wait(barrier, dp - 1 + tp - 1)
-        others(first, lambda target: send_extra(level, target, me).start())
-        for w in range(4):
+            with jax.named_scope("barrier"):
+                pl.semaphore_wait(barrier, dp - 1 + tp - 1)
+        which = range(first, first + count)
+        others(which, lambda g, k: send_extra(level, g, k).start())
+        every(level, 0, which[:1])
+        for w in range(1, 4):
             if first == 0:
                 with jax.named_scope(f"w_in{w}_{level}"):
                     load_in(level, w).wait()
-            part = jnp.dot(gained, w_in[level, w], preferred_element_type=F32)
-            part_send[level, w, span_devices] = part.reshape(
-                count * members, own, cols).astype(BF16)
+            store(w)
             with jax.named_scope(f"send{w}_{level}_{first}"):
-                others(first, lambda target: send_part(level, w, target, me).start())
-        for g in range(first + 1, first + count):
-            others(g, lambda target: send_extra(level, target, me).start())
-            for w in range(4):
-                others(g, lambda target: send_part(level, w, target, me).start())
+                every(level, w, which[:1])
+        for w in range(4):
+            if count > 1:
+                every(level, w, which[1:])
 
     def prepare():
         w_step[:, filled:] = jnp.zeros((layers, LANES - filled, width), BF16)
@@ -329,10 +358,43 @@
         both = fold(
             dp - 1,
             lambda k, sum_in: sum_in + extra_recv[level, k].astype(F32),
-            extra_send[level, me].astype(F32),
+            extra_send[level, mine, place].astype(F32),
         )
         total = both[:, :LANES] + both[:, LANES:]
         scale = lax.rsqrt(total[:, LANES - 1 :] / features + EPS)
+        def await_part(w):
+            with jax.named_scope(f"wr_part{w}_{level}"):
+                arrived(part_recv.at[level, w], part_sem.at[level, w])
+
+        def total_part(w):
+            return scale * fold(
+                dp - 1,
+                lambda k, sum_in: sum_in + part_recv[level, w, k].astype(F32),
+                part_send[level, w, mine, place].astype(F32),
+            )
+
+        fresh_u = {}
+
+        def active(w, j):
+            u = total_part(w).astype(BF16).astype(F32)
+            fresh_u[j] = u
+            return silu(
+                conv_ref[level, j]
+                + u * taps_ref[taps_ref.shape[0] - 1, j, level : level + 1, :].astype(F32))
+
+        load_state(level).wait()
+        await_part(READOUT)
+        cm = active(READOUT, 2)
+        for h in range(heads):
+            window = slice(h // 2 * LANES, h // 2 * LANES + LANES)
+            cm_ref[h] = twice(cm[:, window], h % 2)
+        y = jnp.zeros((heads * own, LANES), F32)
+        for index in range(pieces):
+            window = slice(index * piece, index * piece + piece)
+            read = jnp.concatenate(
+                [state[level, h, :, window] * across(cm_ref, h) for h in range(heads)], axis=0)
+            y = y + jnp.dot(
+                read.astype(BF16), gather[window, :], preferred_element_type=F32)
         chosen = chosen_ref[...]
         high, rest = halves(total * scale)
         raw = jnp.dot(high, chosen, preferred_element_type=F32) + jnp.dot(
@@ -341,38 +403,8 @@
         size = jnp.maximum(raw, 0.0) + jnp.log1p(jnp.exp(-jnp.abs(raw)))
         decay = jnp.exp(-size * params_ref[1, level : level + 1, :])
 
-        def total_part(w):
-            with jax.named_scope(f"wr_part{w}_{level}"):
-                arrived(part_recv.at[level, w], part_sem.at[level, w])
-            return scale * fold(
-                dp - 1,
-                lambda k, sum_in: sum_in + part_recv[level, w, k].astype(F32),
-                part_send[level, w, me].astype(F32),
-            )
-
-        fresh_u = {}
-
-        def active(w, j):
-            u = total_part(w).astype(BF16).astype(F32)
-            fresh_u[j] = u
-            return silu(
-                conv_ref[level, j]
-                + u * taps_ref[taps_ref.shape[0] - 1, j, level : level + 1, :].astype(F32))
-
-        cm = active(READOUT, 2)
-        for h in range(heads):
-            window = slice(h // 2 * LANES, h // 2 * LANES + LANES)
-            cm_ref[h] = twice(cm[:, window], h % 2)
-        with jax.named_scope(f"w_state_{level}"):
-            load_state(level).wait()
-        y = jnp.zeros((heads * own, LANES), F32)
-        with jax.named_scope(f"consult_{level}"):
-            for index in range(pieces):
-                window = slice(index * piece, index * piece + piece)
-                read = jnp.concatenate(
-                    [state[level, h, :, window] * across(cm_ref, h) for h in range(heads)], axis=0)
-                y = y + jnp.dot(
-                    read.astype(BF16), gather[window, :], preferred_element_type=F32)
+        await_part(INMAP)
+        await_part(VALUE)
         bm = active(INMAP, 1)
         for h in range(heads):
             window = slice(h // 2 * LANES, h // 2 * LANES + LANES)
@@ -392,10 +424,11 @@
         y = jnp.concatenate(
             [jnp.where(low, inner[h], inner[h + 1]) for h in range(0, heads, 2)], axis=1)
         y = (y + params_ref[2, level : level + 1, :] * xv) * gain_ref[level : level + 1, :]
+        await_part(GATE)
         gate = total_part(GATE)
-        gated_all[level, me] = (y * silu(gate)).astype(BF16)
+        gated_all[level, mine, place] = (y * silu(gate)).astype(BF16)
         with jax.named_scope(f"s_gated_{level}"):
-            each(dp, lambda k: send_gated(level, source(k), me).start(), 1)
+            others(range(groups), lambda g, k: send_gated(level, g, k).start())
         with jax.named_scope(f"advance_{level}"):
             wide = wide_ref[...].astype(BF16)
 
@@ -424,19 +457,19 @@
         with jax.named_scope(f"wr_gated_{level}_{g}"):
             sem = gated_sem.at[level, g]
             if groups > 1:
-                pl.when(mine == g)(lambda: arrived(gated_all.at[level, : members - 1], sem))
-                pl.when(mine != g)(lambda: arrived(gated_all.at[level, :members], sem))
+                pl.when(mine == g)(lambda: arrived(gated_all.at[level, g, : members - 1], sem))
+                pl.when(mine != g)(lambda: arrived(gated_all.at[level, g], sem))
             else:
-                arrived(gated_all.at[level, : members - 1], sem)
-        gated = gated_all[level, g * members : (g + 1) * members].astype(F32).reshape(rows, cols)
+                arrived(gated_all.at[level, g, : members - 1], sem)
+        gated = gated_all[level, g].astype(F32).reshape(rows, cols)
         square = jnp.sum(gated * gated, axis=1, keepdims=True)
         square_all[level, g, col, :, :rows] = jnp.sum(
             jnp.where(cross, square, 0.0), axis=0, keepdims=True)
-        each(tp - 1, lambda k: send_square(level, g, column(k), col).start())
+        columns(lambda target: send_square(level, g, target, col).start())
         mixed = jnp.dot(gated.astype(BF16), w_out[level], preferred_element_type=F32)
         mixed_all[level, g, col] = mixed.astype(BF16)
         with jax.named_scope(f"s_mixed_{level}_{g}"):
-            each(tp - 1, lambda k: send_mixed(level, g, column(k), col).start())
+            columns(lambda target: send_mixed(level, g, target, col).start())
 
     def renew(level, g):
         arrived(square_all.at[level, g, : tp - 1], square_sem.at[level, g])
@@ -454,17 +487,25 @@
             lambda k, sum_in: sum_in + mixed_all[level, g, k].astype(F32),
             jnp.zeros((rows, width), F32),
         )
-        window = slice(g * rows, (g + 1) * rows)
-        fresh_x = (x_ref[window] + scale * mixed).astype(BF16)
+        fresh_x = (x_ref[g] + scale * mixed).astype(BF16)
         if level == layers - 1:
-            tokens_out[window] = fresh_x
+            for k in range(members):
+                target = (k * groups + g) * own
+                tokens_out[target : target + own] = fresh_x[k * own : (k + 1) * own]
         else:
-            x_ref[window] = fresh_x.astype(F32)
+            x_ref[g] = fresh_x.astype(F32)
 
     prepare()
-    small[0].wait()
-    small[1].wait()
-    x_ref[...] = tokens_ref[...].astype(F32)
+    with jax.named_scope("tokens"):
+        small[0].wait()
+        small[1].wait()
+    load_in(0, 2).start()
+    load_in(0, 3).start()
+    for copy in small[2:]:
+        copy.start()
+    x = tokens_ref[...].astype(F32).reshape(members, groups, own, width)
+    for g in range(groups):
+        x_ref[g] = x[:, g].reshape(rows, width)
     project_in(0, 0, groups)
     load_state(0).start()
     load_out(0).start()
@@ -575,11 +616,11 @@
             pltpu.VMEM((layers, heads, own, entries), F32),
             pltpu.VMEM((LANES, entries), BF16),
             pltpu.VMEM((entries, LANES), BF16),
-            pltpu.VMEM((layers, 4, dp, own, cols), BF16),
+            pltpu.VMEM((layers, 4, groups, dp // groups, own, cols), BF16),
             pltpu.VMEM((layers, 4, dp - 1, own, cols), BF16),
-            pltpu.VMEM((layers, dp, own, 2 * LANES), BF16),
+            pltpu.VMEM((layers, groups, dp // groups, own, 2 * LANES), BF16),
             pltpu.VMEM((layers, dp - 1, own, 2 * LANES), BF16),
-            pltpu.VMEM((layers, dp, own, cols), BF16),
+            pltpu.VMEM((layers, groups, dp // groups, own, cols), BF16),
             pltpu.VMEM((layers, groups, tp, rows, width), BF16),
             pltpu.VMEM((layers, groups, tp, 1, padded), F32),
             pltpu.VMEM((layers, 3, own, cols), F32),
@@ -589,7 +630,7 @@
             pltpu.VMEM((heads, own, LANES), F32),
             pltpu.VMEM((heads, own, LANES), F32),
             pltpu.VMEM((heads * own, LANES), F32),
-            pltpu.VMEM((total, width), F32),
+            pltpu.VMEM((groups, rows, width), F32),
             dma((8,)),
             dma((layers, 4)),
             dma((layers,)),

time: 41 us -> 39.1 us (0.954)
  Pallas kernels: 40.2 us -> 38.3 us
    pallas_call x1, Pallas kernels: 38.4 us -> 36.5 us  [per_device(): pl.pallas_call(functools.partial(kernel, dims), out_shape=(pltpu.VMEM((to...]
where the time goes in v2:
time: 39.1 us; the launch traced here: 38.9 us
  Pallas kernels  38.3 us (98%)
  between operations  0.64 us (2%)
    pallas_call x1, Pallas kernels, per_device(): pl.pallas_call(functools.partial(kernel, dims), out_shape=(pltpu.VMEM((to...  36.5 us
    pallas_call x1, Pallas kernels, per_device(): pl.pallas_call(finish, out_shape=(jax.ShapeDtypeStruct((total, width), BF...  1.79 us

profile of v2, /device:TPU:0, one launch (start us, length us, event | category | flops | bytes accessed | tf_op | source)
XLA Modules:
  0.0 38.9 jit_solution(4796049972559014623)
XLA Ops:
  0.6 36.5 %shard_map.166 = (bf16[64,512]{1,0:T(8,128)(2,1)S(1)}, f32[2,12,8,4096]{3,2,1,0:T(8,128)S(1)}, bf16[2,8,3,4,768]{4,3,2,1,0:T(4,128)(2,1)S(1)}) custom-call(bf16[64,512]{1,0:T(8,128)(2,1)} %tokens_hbm.1, f32[2,512]{1,0:T(2,128)} %norm_hbm.1, f32[2,12]{1,0:T(2,128)} %bias_hbm.1, f32[2,12]{1,0:T(2,128)} %rate_hbm.1, f32[2,12]{1,0:T(2,128)} %skip_hbm.1, ...), custom_call_target="tpu_custom_call" | custom-call | tf_op jit(solution)/shard_map/pallas_call | solution.py:595
  37.1 1.8 %shard_map.167 = (bf16[64,512]{1,0:T(8,128)(2,1)}, f32[2,12,8,4096]{3,2,1,0:T(8,128)}, bf16[2,8,3,4,768]{4,3,2,1,0:T(4,128)(2,1)}) custom-call(bf16[64,512]{1,0:T(8,128)(2,1)S(1)} %get-tuple-element.9.tokens_ref, f32[2,12,8,4096]{3,2,1,0:T(8,128)S(1)} %get-tuple-element.10.fresh_ref, bf16[2,8,3,4,768]{4,3,2,1,0:T(4,128)(2,1)S(1)} %get-tuple-element.11.recent_ref), custom_call_target="tpu_custom_call" | custom-call | tf_op jit(solution)/shard_map/pallas_call | solution.py:665

commit v3 on v2

--- a/solution.py
+++ b/solution.py
@@ -107,7 +107,7 @@
     col = lax.axis_index("tp")
     members = dp // groups
     rows = members * own
-    mine = lax.rem(me, groups)
+    mine = groups - 1 - lax.rem(me, groups)
     place = me // groups
 
     def moved(k):
@@ -118,7 +118,7 @@
             for bit in (1 << power for power in range(members.bit_length() - 1)))
 
     def member(g, k):
-        return moved(k) * groups + g
+        return moved(k) * groups + groups - 1 - g
 
     def slot(g, k):
         return k * groups + lax.rem(g - mine + groups, groups) - 1
@@ -275,14 +275,14 @@
             part_send[level, w, first : first + count] = part.reshape(
                 count, members, own, cols).astype(BF16)
 
-        if first == 0:
+        if level == 0:
             with jax.named_scope(f"w_step_{level}"):
                 load_step(level).wait()
         extra = lax.dot_general(
             gained, w_step[level], (((1,), (1,)), ((), ())), preferred_element_type=F32)
         extra = jnp.where(lane == LANES - 1, square, extra).reshape(count, members, own, LANES)
         high, rest = halves(extra)
-        if first == 0:
+        if level == 0:
             with jax.named_scope(f"w_in0_{level}"):
                 load_in(level, 0).wait()
         extra_send[level, first : first + count, :, :, :LANES] = high
@@ -295,7 +295,7 @@
         others(which, lambda g, k: send_extra(level, g, k).start())
         every(level, 0, which[:1])
         for w in range(1, 4):
-            if first == 0:
+            if level == 0:
                 with jax.named_scope(f"w_in{w}_{level}"):
                     load_in(level, w).wait()
             store(w)
@@ -313,17 +313,16 @@
         which = lax.broadcasted_iota(jnp.int32, (LANES, step), 0)
         entry = lax.broadcasted_iota(jnp.int32, (LANES, step), 1)
         across_lanes = lax.rem(which, head_dim) - entry // span
-        which = lax.broadcasted_iota(jnp.int32, (step, LANES), 1)
-        entry = lax.broadcasted_iota(jnp.int32, (step, LANES), 0)
-        along_rows = lax.rem(which, head_dim) - entry // span
+        which = lax.broadcasted_iota(jnp.int32, gather.shape, 1)
+        entry = lax.broadcasted_iota(jnp.int32, gather.shape, 0)
+        gather[...] = jnp.where(
+            lax.rem(which, gather.shape[0] // span) == entry // span, 1.0, 0.0).astype(BF16)
 
         def fill(index, carry):
             start = pl.multiple_of(index * step, step)
             target = index * (step // span)
             spread[:, pl.ds(start, step)] = jnp.where(
                 across_lanes == target, 1.0, 0.0).astype(BF16)
-            gather[pl.ds(start, step), :] = jnp.where(
-                along_rows == target, 1.0, 0.0).astype(BF16)
             return carry
 
         lax.fori_loop(0, head_dim * span // step, fill, 0)
@@ -355,6 +354,9 @@
     def mix(level):
         with jax.named_scope(f"wr_extra_{level}"):
             arrived(extra_recv.at[level], extra_sem.at[level])
+        load_state(level).wait()
+        with jax.named_scope(f"wr_part0_{level}"):
+            arrived(part_recv.at[level, READOUT], part_sem.at[level, READOUT])
         both = fold(
             dp - 1,
             lambda k, sum_in: sum_in + extra_recv[level, k].astype(F32),
@@ -382,19 +384,22 @@
                 conv_ref[level, j]
                 + u * taps_ref[taps_ref.shape[0] - 1, j, level : level + 1, :].astype(F32))
 
-        load_state(level).wait()
-        await_part(READOUT)
         cm = active(READOUT, 2)
         for h in range(heads):
             window = slice(h // 2 * LANES, h // 2 * LANES + LANES)
             cm_ref[h] = twice(cm[:, window], h % 2)
-        y = jnp.zeros((heads * own, LANES), F32)
-        for index in range(pieces):
-            window = slice(index * piece, index * piece + piece)
-            read = jnp.concatenate(
-                [state[level, h, :, window] * across(cm_ref, h) for h in range(heads)], axis=0)
-            y = y + jnp.dot(
-                read.astype(BF16), gather[window, :], preferred_element_type=F32)
+        doubled = 2 * LANES
+        chunks = head_dim * span // doubled
+        read = jnp.concatenate([
+            state[level, h, :, c * doubled : (c + 1) * doubled]
+            * jnp.concatenate([cm_ref[h]] * 2, axis=1)
+            for c in range(chunks) for h in range(heads)], axis=0).astype(BF16)
+        read = jnp.dot(read, gather[...], preferred_element_type=F32)
+        turn = lax.rem(
+            lax.broadcasted_iota(jnp.int32, (heads * own, LANES), 1), head_dim) // (doubled // span)
+        y = read[: heads * own]
+        for c in range(1, chunks):
+            y = jnp.where(turn == c, read[c * heads * own : (c + 1) * heads * own], y)
         chosen = chosen_ref[...]
         high, rest = halves(total * scale)
         raw = jnp.dot(high, chosen, preferred_element_type=F32) + jnp.dot(
@@ -465,9 +470,9 @@
         square = jnp.sum(gated * gated, axis=1, keepdims=True)
         square_all[level, g, col, :, :rows] = jnp.sum(
             jnp.where(cross, square, 0.0), axis=0, keepdims=True)
-        columns(lambda target: send_square(level, g, target, col).start())
         mixed = jnp.dot(gated.astype(BF16), w_out[level], preferred_element_type=F32)
         mixed_all[level, g, col] = mixed.astype(BF16)
+        columns(lambda target: send_square(level, g, target, col).start())
         with jax.named_scope(f"s_mixed_{level}_{g}"):
             columns(lambda target: send_mixed(level, g, target, col).start())
 
@@ -490,7 +495,7 @@
         fresh_x = (x_ref[g] + scale * mixed).astype(BF16)
         if level == layers - 1:
             for k in range(members):
-                target = (k * groups + g) * own
+                target = (k * groups + groups - 1 - g) * own
                 tokens_out[target : target + own] = fresh_x[k * own : (k + 1) * own]
         else:
             x_ref[g] = fresh_x.astype(F32)
@@ -505,7 +510,7 @@
         copy.start()
     x = tokens_ref[...].astype(F32).reshape(members, groups, own, width)
     for g in range(groups):
-        x_ref[g] = x[:, g].reshape(rows, width)
+        x_ref[g] = x[:, groups - 1 - g].reshape(rows, width)
     project_in(0, 0, groups)
     load_state(0).start()
     load_out(0).start()
@@ -526,6 +531,10 @@
         mix(level)
         for g in range(groups):
             project_out(level, g)
+        if level < layers - 1:
+            load_step(level + 1).wait()
+            for w in range(4):
+                load_in(level + 1, w).wait()
         for g in range(groups):
             renew(level, g)
             if level < layers - 1:
@@ -615,7 +624,7 @@
             pltpu.VMEM((layers, cols, width), BF16),
             pltpu.VMEM((layers, heads, own, entries), F32),
             pltpu.VMEM((LANES, entries), BF16),
-            pltpu.VMEM((entries, LANES), BF16),
+            pltpu.VMEM((2 * LANES, LANES), BF16),
             pltpu.VMEM((layers, 4, groups, dp // groups, own, cols), BF16),
             pltpu.VMEM((layers, 4, dp - 1, own, cols), BF16),
             pltpu.VMEM((layers, groups, dp // groups, own, 2 * LANES), BF16),

time: 39.1 us -> 37.5 us (0.959)
  Pallas kernels: 38.3 us -> 36.7 us
    pallas_call x1, Pallas kernels: 36.5 us -> 34.9 us  [per_device(): pl.pallas_call(functools.partial(kernel, dims), out_shape=(pltpu.VMEM((to...]
where the time goes in v3:
time: 37.5 us; the launch traced here: 37.3 us
  Pallas kernels  36.7 us (98%)
  between operations  0.64 us (2%)
    pallas_call x1, Pallas kernels, per_device(): pl.pallas_call(functools.partial(kernel, dims), out_shape=(pltpu.VMEM((to...  34.9 us
    pallas_call x1, Pallas kernels, per_device(): pl.pallas_call(finish, out_shape=(jax.ShapeDtypeStruct((total, width), BF...  1.79 us

profile of v3, /device:TPU:0, one launch (start us, length us, event | category | flops | bytes accessed | tf_op | source)
XLA Modules:
  0.0 37.3 jit_solution(6163494047331567860)
XLA Ops:
  0.6 34.9 %shard_map.166 = (bf16[64,512]{1,0:T(8,128)(2,1)S(1)}, f32[2,12,8,4096]{3,2,1,0:T(8,128)S(1)}, bf16[2,8,3,4,768]{4,3,2,1,0:T(4,128)(2,1)S(1)}) custom-call(bf16[64,512]{1,0:T(8,128)(2,1)} %tokens_hbm.1, f32[2,512]{1,0:T(2,128)} %norm_hbm.1, f32[2,12]{1,0:T(2,128)} %bias_hbm.1, f32[2,12]{1,0:T(2,128)} %rate_hbm.1, f32[2,12]{1,0:T(2,128)} %skip_hbm.1, ...), custom_call_target="tpu_custom_call" | custom-call | tf_op jit(solution)/shard_map/pallas_call | solution.py:604
  35.5 1.8 %shard_map.167 = (bf16[64,512]{1,0:T(8,128)(2,1)}, f32[2,12,8,4096]{3,2,1,0:T(8,128)}, bf16[2,8,3,4,768]{4,3,2,1,0:T(4,128)(2,1)}) custom-call(bf16[64,512]{1,0:T(8,128)(2,1)S(1)} %get-tuple-element.9.tokens_ref, f32[2,12,8,4096]{3,2,1,0:T(8,128)S(1)} %get-tuple-element.10.fresh_ref, bf16[2,8,3,4,768]{4,3,2,1,0:T(4,128)(2,1)S(1)} %get-tuple-element.11.recent_ref), custom_call_target="tpu_custom_call" | custom-call | tf_op jit(solution)/shard_map/pallas_call | solution.py:674

commit v4 on v3

--- a/solution.py
+++ b/solution.py
@@ -63,9 +63,7 @@
     recent_out,
     tokens_ref,
     norm_ref,
-    bias_ref,
-    rate_ref,
-    skip_ref,
+    head_ref,
     gain_ref,
     taps_ref,
     recent_ref,
@@ -77,8 +75,8 @@
     gather,
     part_send,
     part_recv,
-    extra_send,
-    extra_recv,
+    first_send,
+    first_recv,
     gated_all,
     mixed_all,
     square_all,
@@ -92,11 +90,9 @@
     x_ref,
     small_sem,
     in_sem,
-    step_sem,
-    out_sem,
-    state_sem,
+    bulk_sem,
     send_sem,
-    extra_sem,
+    first_sem,
     part_sem,
     gated_sem,
     mixed_sem,
@@ -138,34 +134,33 @@
         for index, (far, near) in enumerate((
             (tokens_hbm, tokens_ref),
             (norm_hbm, norm_ref),
-            (bias_hbm, bias_ref),
-            (rate_hbm, rate_ref),
-            (skip_hbm, skip_ref),
             (gain_hbm, gain_ref),
             (taps_hbm, taps_ref),
             (recent_hbm, recent_ref),
         ))
     ]
+    heads_sem = small_sem.at[len(small)]
+    per_head = [
+        pltpu.make_async_copy(far, head_ref.at[index], heads_sem)
+        for index, far in enumerate((bias_hbm, rate_hbm, skip_hbm))
+    ]
     sources = (readout_hbm, inmap_hbm, value_hbm, gate_hbm)
     filled = step_hbm.shape[1]
 
-    def load_step(level):
-        return pltpu.make_async_copy(
-            step_hbm.at[level], w_step.at[level, :filled], step_sem.at[level])
+    load_step = pltpu.make_async_copy(step_hbm, w_step.at[:, :filled], bulk_sem.at[0])
+    load_out = pltpu.make_async_copy(project_hbm, w_out, bulk_sem.at[1])
+    load_state = pltpu.make_async_copy(states_hbm, state, bulk_sem.at[2])
 
     def load_in(level, w):
         return pltpu.make_async_copy(
-            sources[w].at[level], w_in.at[level, w], in_sem.at[level, w])
-
-    def load_out(level):
-        return pltpu.make_async_copy(project_hbm.at[level], w_out.at[level], out_sem.at[level])
-
-    def load_state(level):
-        return pltpu.make_async_copy(states_hbm.at[level], state.at[level], state_sem.at[level])
+            sources[w].at[level], w_in.at[level, w], in_sem.at[w if level == 0 else level + 3])
+
+    def await_in(level):
+        pltpu.make_async_copy(w_in.at[level], w_in.at[level], in_sem.at[level + 3]).wait()
 
     for copy in small[:2]:
         copy.start()
-    load_step(0).start()
+    load_step.start()
     load_in(0, 0).start()
     load_in(0, 1).start()
 
@@ -175,22 +170,22 @@
     each(tp - 1, lambda k: pl.semaphore_signal(
         barrier, inc=1, device_id={"tp": column(k)}, device_id_type=MESH))
 
-    def send_extra(level, g, k):
+    def send_first(level, g, k):
         return pltpu.make_async_remote_copy(
-            src_ref=extra_send.at[level, g, moved(k)],
-            dst_ref=extra_recv.at[level, slot(g, k)],
+            src_ref=first_send.at[level, g, moved(k)],
+            dst_ref=first_recv.at[level, slot(g, k)],
             send_sem=send_sem.at[0],
-            recv_sem=extra_sem.at[level],
+            recv_sem=first_sem.at[level],
             device_id={"dp": member(g, k)},
             device_id_type=MESH,
         )
 
     def send_part(level, w, g, k):
         return pltpu.make_async_remote_copy(
-            src_ref=part_send.at[level, w, g, moved(k)],
-            dst_ref=part_recv.at[level, w, slot(g, k)],
+            src_ref=part_send.at[level, w - 1, g, moved(k)],
+            dst_ref=part_recv.at[level, w - 1, slot(g, k)],
             send_sem=send_sem.at[1],
-            recv_sem=part_sem.at[level, w],
+            recv_sem=part_sem.at[level, w // GATE],
             device_id={"dp": member(g, k)},
             device_id_type=MESH,
         )
@@ -240,7 +235,7 @@
             src_ref=ref,
             dst_ref=ref,
             send_sem=send_sem.at[index],
-            recv_sem=extra_sem.at[0],
+            recv_sem=first_sem.at[0],
             device_id={"dp": lax.rem(me + 1, dp)},
             device_id_type=MESH,
         ).wait_send()
@@ -272,12 +267,15 @@
 
         def store(w):
             part = jnp.dot(gained, w_in[level, w], preferred_element_type=F32)
-            part_send[level, w, first : first + count] = part.reshape(
-                count, members, own, cols).astype(BF16)
+            part = part.reshape(count, members, own, cols).astype(BF16)
+            if w == READOUT:
+                first_send[level, first : first + count, :, :, :cols] = part
+            else:
+                part_send[level, w - 1, first : first + count] = part
 
         if level == 0:
             with jax.named_scope(f"w_step_{level}"):
-                load_step(level).wait()
+                load_step.wait()
         extra = lax.dot_general(
             gained, w_step[level], (((1,), (1,)), ((), ())), preferred_element_type=F32)
         extra = jnp.where(lane == LANES - 1, square, extra).reshape(count, members, own, LANES)
@@ -285,15 +283,14 @@
         if level == 0:
             with jax.named_scope(f"w_in0_{level}"):
                 load_in(level, 0).wait()
-        extra_send[level, first : first + count, :, :, :LANES] = high
-        extra_send[level, first : first + count, :, :, LANES:] = rest
+        first_send[level, first : first + count, :, :, cols : cols + LANES] = high
+        first_send[level, first : first + count, :, :, cols + LANES :] = rest
         store(0)
         if level == 0 and first == 0:
             with jax.named_scope("barrier"):
                 pl.semaphore_wait(barrier, dp - 1 + tp - 1)
         which = range(first, first + count)
-        others(which, lambda g, k: send_extra(level, g, k).start())
-        every(level, 0, which[:1])
+        others(which[:1], lambda g, k: send_first(level, g, k).start())
         for w in range(1, 4):
             if level == 0:
                 with jax.named_scope(f"w_in{w}_{level}"):
@@ -301,9 +298,6 @@
             store(w)
             with jax.named_scope(f"send{w}_{level}_{first}"):
                 every(level, w, which[:1])
-        for w in range(4):
-            if count > 1:
-                every(level, w, which[1:])
 
     def prepare():
         w_step[:, filled:] = jnp.zeros((layers, LANES - filled, width), BF16)
@@ -333,7 +327,7 @@
         pick = lax.broadcasted_iota(jnp.int32, (heads, cols), 0)
         slot = lax.broadcasted_iota(jnp.int32, (heads, cols), 1)
         wider = jnp.where(pick == slot // head_dim, 1.0, 0.0)
-        for where, value in enumerate((bias_ref[...], jnp.exp(rate_ref[...]), skip_ref[...])):
+        for where, value in enumerate((head_ref[0], jnp.exp(head_ref[1]), head_ref[2])):
             params_ref[where] = jnp.dot(
                 value, wider, preferred_element_type=F32, precision=lax.Precision.HIGHEST)
 
@@ -353,38 +347,34 @@
 
     def mix(level):
         with jax.named_scope(f"wr_extra_{level}"):
-            arrived(extra_recv.at[level], extra_sem.at[level])
-        load_state(level).wait()
-        with jax.named_scope(f"wr_part0_{level}"):
-            arrived(part_recv.at[level, READOUT], part_sem.at[level, READOUT])
+            arrived(first_recv.at[level], first_sem.at[level])
+        if level == 0:
+            load_state.wait()
         both = fold(
             dp - 1,
-            lambda k, sum_in: sum_in + extra_recv[level, k].astype(F32),
-            extra_send[level, mine, place].astype(F32),
+            lambda k, sum_in: sum_in + first_recv[level, k].astype(F32),
+            first_send[level, mine, place].astype(F32),
         )
-        total = both[:, :LANES] + both[:, LANES:]
+        readout = both[:, :cols]
+        total = both[:, cols : cols + LANES] + both[:, cols + LANES :]
         scale = lax.rsqrt(total[:, LANES - 1 :] / features + EPS)
-        def await_part(w):
-            with jax.named_scope(f"wr_part{w}_{level}"):
-                arrived(part_recv.at[level, w], part_sem.at[level, w])
-
         def total_part(w):
-            return scale * fold(
+            return fold(
                 dp - 1,
-                lambda k, sum_in: sum_in + part_recv[level, w, k].astype(F32),
-                part_send[level, w, mine, place].astype(F32),
+                lambda k, sum_in: sum_in + part_recv[level, w - 1, k].astype(F32),
+                part_send[level, w - 1, mine, place].astype(F32),
             )
 
         fresh_u = {}
 
-        def active(w, j):
-            u = total_part(w).astype(BF16).astype(F32)
+        def active(summed, j):
+            u = (scale * summed).astype(BF16).astype(F32)
             fresh_u[j] = u
             return silu(
                 conv_ref[level, j]
                 + u * taps_ref[taps_ref.shape[0] - 1, j, level : level + 1, :].astype(F32))
 
-        cm = active(READOUT, 2)
+        cm = active(readout, 2)
         for h in range(heads):
             window = slice(h // 2 * LANES, h // 2 * LANES + LANES)
             cm_ref[h] = twice(cm[:, window], h % 2)
@@ -408,14 +398,14 @@
         size = jnp.maximum(raw, 0.0) + jnp.log1p(jnp.exp(-jnp.abs(raw)))
         decay = jnp.exp(-size * params_ref[1, level : level + 1, :])
 
-        await_part(INMAP)
-        await_part(VALUE)
-        bm = active(INMAP, 1)
+        with jax.named_scope(f"wr_part_{level}"):
+            arrived(part_recv.at[level, : GATE - 1], part_sem.at[level, 0])
+        bm = active(total_part(INMAP), 1)
         for h in range(heads):
             window = slice(h // 2 * LANES, h // 2 * LANES + LANES)
             dec_ref[h] = twice(decay[:, window], h % 2)
             bm_ref[h] = twice(bm[:, window], h % 2)
-        xv = active(VALUE, 0)
+        xv = active(total_part(VALUE), 0)
         weighted = size * xv
         inner = []
         for h in range(heads):
@@ -429,8 +419,9 @@
         y = jnp.concatenate(
             [jnp.where(low, inner[h], inner[h + 1]) for h in range(0, heads, 2)], axis=1)
         y = (y + params_ref[2, level : level + 1, :] * xv) * gain_ref[level : level + 1, :]
-        await_part(GATE)
-        gate = total_part(GATE)
+        with jax.named_scope(f"wr_gate_{level}"):
+            arrived(part_recv.at[level, GATE - 1], part_sem.at[level, 1])
+        gate = scale * total_part(GATE)
         gated_all[level, mine, place] = (y * silu(gate)).astype(BF16)
         with jax.named_scope(f"s_gated_{level}"):
             others(range(groups), lambda g, k: send_gated(level, g, k).start())
@@ -457,8 +448,8 @@
         lax.broadcasted_iota(jnp.int32, (rows, rows), 1))
 
     def project_out(level, g):
-        if g == 0:
-            load_out(level).wait()
+        if level == 0 and g == 0:
+            load_out.wait()
         with jax.named_scope(f"wr_gated_{level}_{g}"):
             sem = gated_sem.at[level, g]
             if groups > 1:
@@ -506,41 +497,44 @@
         small[1].wait()
     load_in(0, 2).start()
     load_in(0, 3).start()
-    for copy in small[2:]:
+    for copy in small[2:] + per_head:
         copy.start()
     x = tokens_ref[...].astype(F32).reshape(members, groups, own, width)
     for g in range(groups):
         x_ref[g] = x[:, groups - 1 - g].reshape(rows, width)
     project_in(0, 0, groups)
-    load_state(0).start()
-    load_out(0).start()
+    load_state.start()
+    load_out.start()
     for level in range(1, layers):
-        load_step(level).start()
         for w in range(4):
             load_in(level, w).start()
-        load_state(level).start()
-        load_out(level).start()
+    def rest():
+        if groups > 1:
+            others(range(1, groups), lambda g, k: send_first(0, g, k).start())
+            for w in range(1, 4):
+                every(0, w, range(1, groups))
+
     with jax.named_scope("small_wait"):
         for copy in small[2:]:
             copy.wait()
+        pltpu.make_async_copy(head_ref, head_ref, heads_sem).wait()
     with jax.named_scope("build"):
         build()
         for level in range(layers):
             convolve(level)
+        rest()
     for level in range(layers):
         mix(level)
         for g in range(groups):
             project_out(level, g)
         if level < layers - 1:
-            load_step(level + 1).wait()
-            for w in range(4):
-                load_in(level + 1, w).wait()
+            await_in(level + 1)
         for g in range(groups):
             renew(level, g)
             if level < layers - 1:
                 project_in(level + 1, g, 1)
 
-    sent(extra_recv, 0)
+    sent(first_recv, 0)
     sent(part_recv, 1)
     sent(part_recv.at[:, 0], 2)
     sent(mixed_all.at[:, :, : tp - 1], 3)
@@ -613,9 +607,7 @@
         scratch_shapes=[
             pltpu.VMEM(tokens.shape, BF16),
             pltpu.VMEM(norm_gain.shape, F32),
-            pltpu.VMEM(step_bias.shape, F32),
-            pltpu.VMEM(decay_log.shape, F32),
-            pltpu.VMEM(skip_gain.shape, F32),
+            pltpu.VMEM((3,) + step_bias.shape, F32),
             pltpu.VMEM(gate_gain.shape, F32),
             pltpu.VMEM(taps.shape, BF16),
             pltpu.VMEM(turned.shape, BF16),
@@ -625,10 +617,10 @@
             pltpu.VMEM((layers, heads, own, entries), F32),
             pltpu.VMEM((LANES, entries), BF16),
             pltpu.VMEM((2 * LANES, LANES), BF16),
-            pltpu.VMEM((layers, 4, groups, dp // groups, own, cols), BF16),
-            pltpu.VMEM((layers, 4, dp - 1, own, cols), BF16),
-            pltpu.VMEM((layers, groups, dp // groups, own, 2 * LANES), BF16),
-            pltpu.VMEM((layers, dp - 1, own, 2 * LANES), BF16),
+            pltpu.VMEM((layers, 3, groups, dp // groups, own, cols), BF16),
+            pltpu.VMEM((layers, 3, dp - 1, own, cols), BF16),
+            pltpu.VMEM((layers, groups, dp // groups, own, cols + 2 * LANES), BF16),
+            pltpu.VMEM((layers, dp - 1, own, cols + 2 * LANES), BF16),
             pltpu.VMEM((layers, groups, dp // groups, own, cols), BF16),
             pltpu.VMEM((layers, groups, tp, rows, width), BF16),
             pltpu.VMEM((layers, groups, tp, 1, padded), F32),
@@ -640,14 +632,12 @@
             pltpu.VMEM((heads, own, LANES), F32),
             pltpu.VMEM((heads * own, LANES), F32),
             pltpu.VMEM((groups, rows, width), F32),
-            dma((8,)),
-            dma((layers, 4)),
-            dma((layers,)),
-            dma((layers,)),
-            dma((layers,)),
+            dma((6,)),
+            dma((layers + 3,)),
+            dma((3,)),
             dma((5,)),
             dma((layers,)),
-            dma((layers, 4)),
+            dma((layers, 2)),
             dma((layers, groups)),
             dma((layers, groups)),
             dma((layers, groups)),

time: 37.5 us -> 36.9 us (0.984)
  Pallas kernels: 36.7 us -> 36.1 us
    pallas_call x1, Pallas kernels: 34.9 us -> 34.3 us  [per_device(): pl.pallas_call(functools.partial(kernel, dims), out_shape=(pltpu.VMEM((to...]
where the time goes in v4:
time: 36.9 us; the launch traced here: 36.8 us
  Pallas kernels  36.1 us (98%)
  between operations  0.64 us (2%)
    pallas_call x1, Pallas kernels, per_device(): pl.pallas_call(functools.partial(kernel, dims), out_shape=(pltpu.VMEM((to...  34.3 us
    pallas_call x1, Pallas kernels, per_device(): pl.pallas_call(finish, out_shape=(jax.ShapeDtypeStruct((total, width), BF...  1.79 us

profile of v4, /device:TPU:0, one launch (start us, length us, event | category | flops | bytes accessed | tf_op | source)
XLA Modules:
  0.0 36.8 jit_solution(13639195431816005358)
XLA Ops:
  0.6 34.3 %shard_map.166 = (bf16[64,512]{1,0:T(8,128)(2,1)S(1)}, f32[2,12,8,4096]{3,2,1,0:T(8,128)S(1)}, bf16[2,8,3,4,768]{4,3,2,1,0:T(4,128)(2,1)S(1)}) custom-call(bf16[64,512]{1,0:T(8,128)(2,1)} %tokens_hbm.1, f32[2,512]{1,0:T(2,128)} %norm_hbm.1, f32[2,12]{1,0:T(2,128)} %bias_hbm.1, f32[2,12]{1,0:T(2,128)} %rate_hbm.1, f32[2,12]{1,0:T(2,128)} %skip_hbm.1, ...), custom_call_target="tpu_custom_call" | custom-call | tf_op jit(solution)/shard_map/pallas_call | solution.py:598
  35.0 1.8 %shard_map.167 = (bf16[64,512]{1,0:T(8,128)(2,1)}, f32[2,12,8,4096]{3,2,1,0:T(8,128)}, bf16[2,8,3,4,768]{4,3,2,1,0:T(4,128)(2,1)}) custom-call(bf16[64,512]{1,0:T(8,128)(2,1)S(1)} %get-tuple-element.9.tokens_ref, f32[2,12,8,4096]{3,2,1,0:T(8,128)S(1)} %get-tuple-element.10.fresh_ref, bf16[2,8,3,4,768]{4,3,2,1,0:T(4,128)(2,1)S(1)} %get-tuple-element.11.recent_ref), custom_call_target="tpu_custom_call" | custom-call | tf_op jit(solution)/shard_map/pallas_call | solution.py:664

commit v5 on v4

--- a/solution.py
+++ b/solution.py
@@ -158,17 +158,17 @@
     def await_in(level):
         pltpu.make_async_copy(w_in.at[level], w_in.at[level], in_sem.at[level + 3]).wait()
 
+    barrier = pltpu.get_barrier_semaphore()
+    each(dp, lambda k: pl.semaphore_signal(
+        barrier, inc=1, device_id={"dp": lax.rem(me + k, dp)}, device_id_type=MESH), 1)
+    each(tp - 1, lambda k: pl.semaphore_signal(
+        barrier, inc=1, device_id={"tp": column(k)}, device_id_type=MESH))
+
     for copy in small[:2]:
         copy.start()
     load_step.start()
     load_in(0, 0).start()
     load_in(0, 1).start()
-
-    barrier = pltpu.get_barrier_semaphore()
-    each(dp, lambda k: pl.semaphore_signal(
-        barrier, inc=1, device_id={"dp": lax.rem(me + k, dp)}, device_id_type=MESH), 1)
-    each(tp - 1, lambda k: pl.semaphore_signal(
-        barrier, inc=1, device_id={"tp": column(k)}, device_id_type=MESH))
 
     def send_first(level, g, k):
         return pltpu.make_async_remote_copy(
@@ -425,24 +425,27 @@
         gated_all[level, mine, place] = (y * silu(gate)).astype(BF16)
         with jax.named_scope(f"s_gated_{level}"):
             others(range(groups), lambda g, k: send_gated(level, g, k).start())
-        with jax.named_scope(f"advance_{level}"):
-            wide = wide_ref[...].astype(BF16)
-
-            def advance(index, carry):
-                window = pl.ds(pl.multiple_of(index * piece, piece), piece)
-                grown = jnp.dot(wide, spread[:, window], preferred_element_type=F32)
-                for h in range(heads):
-                    fresh_out[level, h, :, window] = (
-                        across(dec_ref, h) * state[level, h, :, window]
-                        + grown[h * own : (h + 1) * own] * across(bm_ref, h))
-                return carry
-
-            lax.fori_loop(0, pieces, advance, 0)
-        with jax.named_scope(f"recent_{level}"):
-            for j in range(3):
-                kept = recent_ref[level, :, j].astype(F32)
-                recent_out[level, :, j] = jnp.concatenate(
-                    [kept[:, 1:], fresh_u[j][:, None]], axis=1).astype(BF16)
+        def settle():
+            with jax.named_scope(f"advance_{level}"):
+                wide = wide_ref[...].astype(BF16)
+
+                def advance(index, carry):
+                    window = pl.ds(pl.multiple_of(index * piece, piece), piece)
+                    grown = jnp.dot(wide, spread[:, window], preferred_element_type=F32)
+                    for h in range(heads):
+                        fresh_out[level, h, :, window] = (
+                            across(dec_ref, h) * state[level, h, :, window]
+                            + grown[h * own : (h + 1) * own] * across(bm_ref, h))
+                    return carry
+
+                lax.fori_loop(0, pieces, advance, 0)
+            with jax.named_scope(f"recent_{level}"):
+                for j in range(3):
+                    kept = recent_ref[level, :, j].astype(F32)
+                    recent_out[level, :, j] = jnp.concatenate(
+                        [kept[:, 1:], fresh_u[j][:, None]], axis=1).astype(BF16)
+
+        return settle
 
     cross = lax.broadcasted_iota(jnp.int32, (rows, rows), 0) == (
         lax.broadcasted_iota(jnp.int32, (rows, rows), 1))
@@ -524,9 +527,14 @@
             convolve(level)
         rest()
     for level in range(layers):
-        mix(level)
+        settle = mix(level)
+        late = level < layers - 1 and groups > 1
+        if not late:
+            settle()
         for g in range(groups):
             project_out(level, g)
+            if late and g == 0:
+                settle()
         if level < layers - 1:
             await_in(level + 1)
         for g in range(groups):

time: 36.9 us -> 36.3 us (0.984)
  Pallas kernels: 36.1 us -> 35.4 us
    pallas_call x1, Pallas kernels: 34.3 us -> 33.7 us  [per_device(): pl.pallas_call(functools.partial(kernel, dims), out_shape=(pltpu.VMEM((to...]
where the time goes in v5:
time: 36.3 us; the launch traced here: 36.1 us
  Pallas kernels  35.4 us (98%)
  between operations  0.64 us (2%)
    pallas_call x1, Pallas kernels, per_device(): pl.pallas_call(functools.partial(kernel, dims), out_shape=(pltpu.VMEM((to...  33.7 us
    pallas_call x1, Pallas kernels, per_device(): pl.pallas_call(finish, out_shape=(jax.ShapeDtypeStruct((total, width), BF...  1.79 us

profile of v5, /device:TPU:0, one launch (start us, length us, event | category | flops | bytes accessed | tf_op | source)
XLA Modules:
  0.0 36.1 jit_solution(9573222860056438041)
XLA Ops:
  0.6 33.7 %shard_map.166 = (bf16[64,512]{1,0:T(8,128)(2,1)S(1)}, f32[2,12,8,4096]{3,2,1,0:T(8,128)S(1)}, bf16[2,8,3,4,768]{4,3,2,1,0:T(4,128)(2,1)S(1)}) custom-call(bf16[64,512]{1,0:T(8,128)(2,1)} %tokens_hbm.1, f32[2,512]{1,0:T(2,128)} %norm_hbm.1, f32[2,12]{1,0:T(2,128)} %bias_hbm.1, f32[2,12]{1,0:T(2,128)} %rate_hbm.1, f32[2,12]{1,0:T(2,128)} %skip_hbm.1, ...), custom_call_target="tpu_custom_call" | custom-call | tf_op jit(solution)/shard_map/pallas_call | solution.py:606
  34.3 1.8 %shard_map.167 = (bf16[64,512]{1,0:T(8,128)(2,1)}, f32[2,12,8,4096]{3,2,1,0:T(8,128)}, bf16[2,8,3,4,768]{4,3,2,1,0:T(4,128)(2,1)}) custom-call(bf16[64,512]{1,0:T(8,128)(2,1)S(1)} %get-tuple-element.9.tokens_ref, f32[2,12,8,4096]{3,2,1,0:T(8,128)S(1)} %get-tuple-element.10.fresh_ref, bf16[2,8,3,4,768]{4,3,2,1,0:T(4,128)(2,1)S(1)} %get-tuple-element.11.recent_ref), custom_call_target="tpu_custom_call" | custom-call | tf_op jit(solution)/shard_map/pallas_call | solution.py:672
